TPU v7x, 32 devices: a whole 2x2x4 slice. The times are simulated.
32 devices in a mesh: sp: 8 (over z, x), tp: 4 (over y, core).
Axes of the slice: x: 2, y: 2, z: 4, core: 2. Of those that a mesh axis runs over, the one named last changes fastest.
Arguments:
- wide_query: bfloat16 [4096, 1536], P('sp', 'tp'), may hold values from -6 to 6
- wide_key: bfloat16 [4096, 1536], P('sp', 'tp'), may hold values from -6 to 6
- wide_value: bfloat16 [4096, 1536], P('sp', 'tp'), may hold values from -6 to 6
- wide_gate: bfloat16 [4096, 1536], P('sp', 'tp'), may hold values from -6 to 6
- narrow_query: bfloat16 [4096, 512], P('sp', 'tp'), may hold values from -6 to 6
- narrow_key: bfloat16 [4096, 512], P('sp', 'tp'), may hold values from -6 to 6
- narrow_value: bfloat16 [4096, 512], P('sp', 'tp'), may hold values from -6 to 6
- narrow_gate: bfloat16 [4096, 512], P('sp', 'tp'), may hold values from -6 to 6
- wide_decay: float32 [12, 4096], P('tp', 'sp'), may hold values from -1 to 0
- narrow_decay: float32 [8, 4096], P('tp', 'sp'), may hold values from -1 to 0
- residual: bfloat16 [4096, 2048], P(('sp', 'tp')), may hold values from -6 to 6
- wide_out: bfloat16 [1536, 2048], P('tp'), may hold values from -0.125 to 0.125
- narrow_out: bfloat16 [512, 2048], P('tp'), may hold values from -0.125 to 0.125
- up_weight: bfloat16 [2048, 8192], P('sp', 'tp'), may hold values from -0.125 to 0.125
- down_weight: bfloat16 [8192, 2048], P('tp', 'sp'), may hold values from -0.0625 to 0.0625
- gain_mix: float32 [2048], replicated, may hold values from 0.1 to 1.9
- gain_pre: float32 [2048], replicated, may hold values from 0.1 to 1.9
- gain_mlp: float32 [2048], replicated, may hold values from 0.1 to 1.9
Outputs:
- result: bfloat16 [4096, 2048], P(('sp', 'tp'))
All inputs are finite; a program needn't handle non-finite values.
Results may differ from a plain program's by a relative error of at most 0.02.
Values may be sent and summed in bfloat16 or wider, within the bound.
A program may use at most 128 MiB of HBM per device.

v0:
```python
import jax
import jax.numpy as jnp
from jax import lax
from jax.sharding import PartitionSpec as P

WIDE_DIM = 128
NARROW_DIM = 64
SPAN = 128


epsilon = 1e-06


def prefix_2(array, axis, join, neutral):
    place = lax.axis_index(axis)
    gathered = jax.tree.map(
        lambda a, kind: lax.all_gather(a.astype(kind), axis),
        array,
        (jnp.bfloat16, jnp.bfloat16, jnp.bfloat16, jnp.bfloat16),
    )
    state = jax.tree.map(lambda a, e: jnp.zeros_like(a) + jnp.asarray(e, a.dtype), array, neutral)

    def one(turn, state):
        return join(
            state,
            jax.tree.map(
                lambda a, own: lax.dynamic_index_in_dim(a, turn, 0, False).astype(own.dtype),
                gathered,
                array,
            ),
        )

    return lax.fori_loop(0, place, one, state)


def rotate(packed, head_dim, positions):
    length = packed.shape[0]
    grouped = packed.astype(jnp.float32).reshape(length, -1, head_dim)
    halfway = head_dim // 2
    inverse = 10000.0 ** (-jnp.arange(0, head_dim, 2, dtype=jnp.float32) / head_dim)
    angles = positions.astype(jnp.float32)[:, None] * inverse[None, :]
    cosine_table = jnp.cos(angles)[:, None, :]
    sine_table = jnp.sin(angles)[:, None, :]
    leading = grouped[..., :halfway]
    trailing = grouped[..., halfway:]
    return jnp.concatenate(
        [
            leading * cosine_table - trailing * sine_table,
            leading * sine_table + trailing * cosine_table,
        ],
        axis=-1,
    )


def rms_scale(values, gain_vector):
    return (
        values
        * lax.rsqrt(jnp.mean(values * values, axis=-1, keepdims=True) + epsilon)
        * gain_vector
    )


def span_terms(query, key, value, log_decay, head_dim, offset):
    length = query.shape[0]
    count_of_heads = query.shape[1] // head_dim
    span_count = length // SPAN
    shaped = (span_count, SPAN, count_of_heads, head_dim)
    positions = offset + jnp.arange(length, dtype=jnp.int32)
    queries = rotate(query, head_dim, positions).astype(jnp.bfloat16).reshape(shaped)
    keys_full = (rotate(key, head_dim, positions) * head_dim ** (-0.5)).reshape(shaped)
    keys_half = keys_full.astype(jnp.bfloat16)
    values_all = value.reshape(shaped)
    cumulative = jnp.cumsum(log_decay.T.reshape(span_count, SPAN, count_of_heads), axis=1)
    causal = jnp.arange(SPAN)[:, None] >= jnp.arange(SPAN)[None, :]
    scores = jnp.einsum("nihd,njhd->nhij", queries, keys_half, preferred_element_type=jnp.float32)
    decay_rows = cumulative.transpose(0, 2, 1)
    log_gaps = jnp.where(causal, decay_rows[..., :, None] - decay_rows[..., None, :], -jnp.inf)
    weights = (scores * jnp.exp(log_gaps)).astype(jnp.bfloat16)
    within = jnp.einsum("nhij,njhd->nihd", weights, values_all, preferred_element_type=jnp.float32)
    span_total = cumulative[:, -1, :]
    scaled = (keys_full * jnp.exp(span_total[:, None, :] - cumulative)[..., None]).astype(
        jnp.bfloat16
    )
    own_state = jnp.einsum(
        "njhd,njhe->nhde", scaled, values_all, preferred_element_type=jnp.float32
    )

    def advance(carried, inputs):
        decay_sum, contribution = inputs
        return (carried * jnp.exp(decay_sum)[:, None, None] + contribution, carried)

    initial = jnp.zeros((count_of_heads, head_dim, head_dim), jnp.float32)
    closing, before = lax.scan(advance, initial, (span_total, own_state))
    device_decay = jnp.exp(jnp.sum(span_total, axis=0))
    return (queries, cumulative, within, span_total, before, closing, device_decay)


def finish(parts, prefix, gate, head_dim):
    queries, cumulative, within, span_total, before, closing, device_decay = parts
    length = gate.shape[0]
    earlier = jnp.cumsum(span_total, axis=0) - span_total
    entering = (prefix[None] * jnp.exp(earlier)[:, :, None, None] + before).astype(jnp.bfloat16)
    across = (
        jnp.einsum("nihd,nhde->nihe", queries, entering, preferred_element_type=jnp.float32)
        * jnp.exp(cumulative)[..., None]
    )
    output = (within + across).reshape(length, -1, head_dim)
    normed = output * lax.rsqrt(jnp.mean(output * output, axis=-1, keepdims=True) + epsilon)
    return (normed.reshape(length, -1) * jax.nn.silu(gate.astype(jnp.float32))).astype(jnp.bfloat16)


def combine_states(former, latter):
    return (
        former[0] * latter[0],
        former[1] * latter[0][:, None, None] + latter[1],
        former[2] * latter[2],
        former[3] * latter[2][:, None, None] + latter[3],
    )


def local(
    wide_query,
    wide_key,
    wide_value,
    wide_gate,
    narrow_query,
    narrow_key,
    narrow_value,
    narrow_gate,
    wide_decay,
    narrow_decay,
    residual,
    wide_out,
    narrow_out,
    up_weight,
    down_weight,
    gain_mix,
    gain_pre,
    gain_mlp,
):
    length = wide_query.shape[0]
    offset = lax.axis_index("sp") * length
    wide_parts = span_terms(wide_query, wide_key, wide_value, wide_decay, WIDE_DIM, offset)
    narrow_parts = span_terms(
        narrow_query, narrow_key, narrow_value, narrow_decay, NARROW_DIM, offset
    )
    identity = (
        jnp.ones_like(wide_parts[6]),
        jnp.zeros_like(wide_parts[5]),
        jnp.ones_like(narrow_parts[6]),
        jnp.zeros_like(narrow_parts[5]),
    )
    prefixes = prefix_2(
        (wide_parts[6], wide_parts[5], narrow_parts[6], narrow_parts[5]),
        "sp",
        combine_states,
        identity,
    )
    wide_mixed = finish(wide_parts, prefixes[1], wide_gate, WIDE_DIM)
    narrow_mixed = finish(narrow_parts, prefixes[3], narrow_gate, NARROW_DIM)
    wide_rows, narrow_rows = (
        lax.all_to_all(wide_mixed, "tp", split_axis=0, concat_axis=1, tiled=True),
        lax.all_to_all(narrow_mixed, "tp", split_axis=0, concat_axis=1, tiled=True),
    )
    wide_whole, narrow_whole = (
        lax.all_gather(wide_out, "tp", axis=0, tiled=True),
        lax.all_gather(narrow_out, "tp", axis=0, tiled=True),
    )
    projected = jnp.dot(wide_rows, wide_whole, preferred_element_type=jnp.float32) + jnp.dot(
        narrow_rows, narrow_whole, preferred_element_type=jnp.float32
    )
    updated = (residual.astype(jnp.float32) + rms_scale(projected, gain_mix)).astype(jnp.bfloat16)
    normed = rms_scale(updated.astype(jnp.float32), gain_pre).astype(jnp.bfloat16)
    block_rows = lax.all_gather(normed, "tp", axis=0, tiled=True)
    rectified = jax.nn.relu(
        jnp.dot(
            block_rows,
            lax.all_gather(up_weight, "sp", axis=0, tiled=True),
            preferred_element_type=jnp.float32,
        )
    )
    hidden = (rectified * rectified).astype(jnp.bfloat16)
    partial_terms = jnp.dot(
        hidden,
        lax.all_gather(down_weight, "sp", axis=1, tiled=True),
        preferred_element_type=jnp.float32,
    )
    lowered = lax.psum_scatter(
        partial_terms.astype(jnp.bfloat16), "tp", scatter_dimension=0, tiled=True
    ).astype(jnp.float32)
    return (updated.astype(jnp.float32) + rms_scale(lowered, gain_mlp)).astype(jnp.bfloat16)


def solution(mesh):
    return jax.shard_map(
        local,
        mesh=mesh,
        in_specs=(
            P("sp", "tp"),
            P("sp", "tp"),
            P("sp", "tp"),
            P("sp", "tp"),
            P("sp", "tp"),
            P("sp", "tp"),
            P("sp", "tp"),
            P("sp", "tp"),
            P("tp", "sp"),
            P("tp", "sp"),
            P(("sp", "tp"), None),
            P("tp", None),
            P("tp", None),
            P("sp", "tp"),
            P("tp", "sp"),
            P(),
            P(),
            P(),
        ),
        out_specs=P(("sp", "tp"), None),
        check_vma=False,
    )
```

profile of v0, /device:TPU:25, one launch (start us, length us, event | category | flops | bytes accessed | tf_op | source)
XLA Modules:
  0.0 505.8 jit_solution(15633803309684791243)
XLA Ops:
  6.5 0.7 all-gather.10.cloned.1.call-update
  7.3 0.7 all-gather.12.cloned.1.call-update
  8.1 1.2 copy.77
  10.2 1.0 subtract_convert_fusion
  12.6 0.8 fusion.76
  13.6 0.8 fusion.33
  14.4 3.3 while.42
  14.4 0.7 bitcast_dynamic-update-slice_fusion.8
  15.2 0.7 bitcast_dynamic-update-slice_fusion.8
  16.0 0.7 bitcast_dynamic-update-slice_fusion.8
  16.9 0.7 bitcast_dynamic-update-slice_fusion.8
  17.7 24.6 %all-gather.1 = bf16[24,128,128]{2,1,0:T(8,128)(2,1)S(1)} all-gather(bf16[3,128,128]{2,1,0:T(8,128)(2,1)S(1)} %convert_element_type.154), channel_id=3, replica_groups=mesh['sp'=8,'tp'=4] {'sp'}, dimensions={0}, use_global_device_ids=true | all-gather | bytes 884736 | tf_op jit(solution)/shard_map/all_gather | solution.py:17
  42.4 1.0 multiply_cosine_fusion.1
  43.3 1.7 copy.93
  45.0 0.9 convert.30
  45.9 1.7 copy.106
  47.6 0.9 convert.31
  48.5 1.6 fusion.61
  50.2 0.7 bitcast_dynamic-update-slice_fusion.3
  50.9 0.9 copy.122
  51.7 1.2 reduce_window_sum.45
  53.8 0.9 fusion.74
  54.7 1.1 copy.97
  55.7 1.8 reshape.384
  57.5 1.7 copy.99
  59.2 1.6 bitcast_dynamic-update-slice_fusion.2
  60.8 1.9 fusion.54
  62.7 6.2 %while.43 = (s32[]{:T(128)}, f32[2,64,64]{2,1,0:T(8,128)S(1)}, f32[4,2,64,64]{3,2,1,0:T(8,128)}, f32[4,2]{1,0:T(4,128)S(1)}, f32[4,2,64,64]{3,2,1,0:T(8,128)}, /*index=5*/s32[]{:T(128)}, s32[]{:T(128)}) while((s32[]{:T(128)}, f32[2,64,64]{2,1,0:T(8,128)S(1)}, f32[4,2,64,64]{3,2,1,0:T(8,128)}, f32[4,2]{1,0:T(4,128)S(1)}, ...), condition=%wide.region_7.8_spmd.clone, body=%wide.region_6.7_spmd.clone.sunk | while | flops 32771 | bytes 197240 | solution.py:93
  63.3 0.9 bitcast_add_fusion.5
  64.9 0.9 bitcast_add_fusion.5
  66.4 0.9 bitcast_add_fusion.5
  68.0 0.9 bitcast_add_fusion.5
  68.9 26.1 %all-gather.3 = bf16[16,64,64]{2,1,0:T(8,128)(2,1)} all-gather(bf16[2,64,64]{2,1,0:T(8,128)(2,1)S(1)} %convert_element_type.158), channel_id=5, replica_groups=mesh['sp'=8,'tp'=4] {'sp'}, dimensions={0}, use_global_device_ids=true | all-gather | bytes 147456 | tf_op jit(solution)/shard_map/all_gather | solution.py:17
  95.7 1.3 dynamic-slice
  98.7 15.3 %all-reduce.2 = (bf16[24]{0:T(256)(128)(2,1)S(1)}, bf16[16]{0:T(256)(128)(2,1)S(1)}) all-reduce(bf16[24]{0:T(256)(128)(2,1)S(1)} %dynamic-update-slice, bf16[16]{0:T(256)(128)(2,1)S(1)} %dynamic-update-slice.1), channel_id=2, replica_groups=mesh['sp'=8,'tp'=4] {'sp'}, use_global_device_ids=true, to_apply=%add | all-reduce | flops 40 | bytes 160
  114.3 5.9 %while.41 = (s32[]{:T(128)}, f32[3,128,128]{2,1,0:T(8,128)S(1)}, f32[2,64,64]{2,1,0:T(8,128)S(1)}, s32[]{:T(128)}, bf16[8,3]{1,0:T(8,128)(2,1)S(1)}, /*index=5*/...) while((s32[]{:T(128)}, f32[3,128,128]{2,1,0:T(8,128)S(1)}, ...), condition=%wide.region_9.10_spmd, body=%wide.region_8.9_spmd.sunk | while | flops 172042 | bytes 573649 | solution.py:33
  114.4 0.8 convert_add_fusion.6
  115.4 0.8 convert_add_fusion.6
  116.4 0.8 convert_add_fusion.6
  117.4 0.8 convert_add_fusion.6
  118.3 0.8 convert_add_fusion.6
  119.3 0.8 convert_add_fusion.6
  120.1 1.0 concatenate.34
  121.4 1.7 concatenate.35
  123.1 1.2 copy.79
  124.2 1.1 copy.102
  126.1 2.6 fusion.8
  128.6 3.1 multiply_reduce_fusion.1
  131.8 1.7 copy.103
  133.5 1.2 copy.104
  134.9 0.8 copy_bitcast_fusion
  135.8 19.7 %all-to-all-start = ((bf16[4,128,384]{1,2,0:T(8,128)(2,1)}), bf16[4,128,384]{1,2,0:T(8,128)(2,1)S(1)}, u32[]{:S(2)}, u32[]{:S(2)}) async-start(bf16[4,128,384]{1,2,0:T(8,128)(2,1)} %copy_bitcast_fusion), calls=%async_computation | async-start | bytes 786432 | tf_op jit(solution)/shard_map/all_to_all | solution.py:162
  158.0 3.9 all-to-all-done
  161.9 4.3 all-to-all-start.1
  166.2 3.8 fusion.77
  170.0 2.2 multiply_reduce_fusion
  172.7 1.0 fusion.20
  174.9 23.7 %all-gather.14.cloned.1.call-done = bf16[512,2048]{1,0:T(8,128)(2,1)} async-done(((bf16[128,2048]{1,0:T(8,128)(2,1)}), bf16[512,2048]{1,0:T(8,128)(2,1)}) %all-gather.14.cloned.1.call-update) | async-done | bytes 2097168 | tf_op jit(solution)/shard_map/all_gather | solution.py:174
  198.6 124.3 %all-gather.16.cloned.1.call-done = bf16[2048,2048]{1,0:T(8,128)(2,1)} async-done(((bf16[256,2048]{1,0:T(8,128)(2,1)}), bf16[2048,2048]{1,0:T(8,128)(2,1)}) %all-gather.16.cloned.1.call-update) | async-done | bytes 8388624 | tf_op jit(solution)/shard_map/all_gather | solution.py:178
  322.9 125.1 %all-gather.18.cloned.1.call-done = bf16[2048,2048]{1,0:T(8,128)(2,1)} async-done(((bf16[2048,256]{1,0:T(8,128)(2,1)}), bf16[2048,2048]{1,0:T(8,128)(2,1)}) %all-gather.18.cloned.1.call-update) | async-done | bytes 8388624 | tf_op jit(solution)/shard_map/all_gather | solution.py:185
  447.9 16.5 %convolution_convert_fusion = bf16[512,2048]{1,0:T(8,128)(2,1)} fusion(bf16[2048,2048]{1,0:T(8,128)(2,1)} %all-gather.18.cloned.1.call-done, bf16[512,2048]{1,0:T(8,128)(2,1)} %all-gather.14.cloned.1.call-done, bf16[2048,2048]{1,0:T(8,128)(2,1)} %all-gather.16.cloned.1.call-done), kind=kOutput, calls=%fused_computation.19 | convolution fusion | flops 8594128896 | bytes 20971520 | tf_op jit(solution)/shard_map/dot_general | solution.py:183
  464.4 31.2 %reduce-scatter.2.cloned.1.call-done = bf16[128,2048]{1,0:T(8,128)(2,1)} async-done(((bf16[512,2048]{1,0:T(8,128)(2,1)}), bf16[128,2048]{1,0:T(8,128)(2,1)}) %reduce-scatter.2.cloned.1.call-update) | async-done | bytes 524304 | tf_op jit(solution)/shard_map/reduce_scatter | solution.py:188
  495.6 1.2 fusion.16
  496.9 2.1 fusion.21
  (145 shorter events, 13.8 us)
Async XLA Ops:
  6.5 2.8 copy-start.7
  6.5 159.6 %all-gather.10.cloned.1.call-start = ((), (), s32[]{:S(2)}) async-start(), calls=%async_computation.3 | async-start | bytes 7864320 | tf_op jit(solution)/shard_map/all_gather | solution.py:166
  7.3 162.8 %all-gather.12.cloned.1.call-start = ((), (), s32[]{:S(2)}) async-start(), calls=%async_computation.4 | async-start | bytes 2621440 | tf_op jit(solution)/shard_map/all_gather | solution.py:167
  9.6 2.5 copy-start.17
  10.2 3.2 copy-start.6
  14.4 36.5 %copy-start.18 = (f32[2,512]{1,0:T(2,128)S(1)}, f32[2,512]{1,0:T(2,128)}, u32[]{:S(2)}) copy-start(f32[2,512]{1,0:T(2,128)} %param.33) | copy-start | bytes 12292
  53.0 61.3 %copy-start = (f32[4,128,2]{2,1,0:T(8,128)}, f32[4,128,2]{2,1,0:T(8,128)S(1)}, u32[]{:S(2)}) copy-start(f32[4,128,2]{2,1,0:T(8,128)S(1)} %reduce_window_sum.45) | copy-start | bytes 12292
  53.7 1.0 copy-start.12
  128.6 27.2 %copy-start.1 = (f32[4,128,2]{2,1,0:T(8,128)S(1)}, f32[4,128,2]{2,1,0:T(8,128)}, u32[]{:S(2)}) copy-start(f32[4,128,2]{2,1,0:T(8,128)} %copy-done) | copy-start | bytes 12292
  128.6 27.3 %copy-start.8 = (bf16[2,4,4,8,128]{4,3,2,1,0:T(8,128)(2,1)S(1)}, bf16[2,4,4,8,128]{4,3,2,1,0:T(8,128)(2,1)}, u32[]{:S(2)}) copy-start(bf16[2,4,4,8,128]{4,3,2,1,0:T(8,128)(2,1)} %get-tuple-element.233) | copy-start | bytes 196612
  131.7 23.8 %copy-start.13 = (f32[4,1,2]{0,2,1:T(2,128)S(1)}, f32[4,1,2]{0,2,1:T(2,128)}, u32[]{:S(2)}) copy-start(f32[4,1,2]{0,2,1:T(2,128)} %copy-done.12) | copy-start | bytes 100
  131.7 23.9 %copy-start.2 = (f32[4,128,2]{2,1,0:T(8,128)S(1)}, f32[4,128,2]{2,1,0:T(8,128)}, u32[]{:S(2)}) copy-start(f32[4,128,2]{2,1,0:T(8,128)} %get-tuple-element.236) | copy-start | bytes 12292
  131.7 24.3 %copy-start.9 = (f32[4,2,64,64]{3,2,1,0:T(8,128)S(1)}, f32[4,2,64,64]{3,2,1,0:T(8,128)}, u32[]{:S(2)}) copy-start(f32[4,2,64,64]{3,2,1,0:T(8,128)} %get-tuple-element.136) | copy-start | bytes 393220
  131.7 24.6 %copy-start.3 = (f32[4,128,2,64]{1,3,2,0:T(8,128)S(1)}, f32[4,128,2,64]{1,3,2,0:T(8,128)}, u32[]{:S(2)}) copy-start(f32[4,128,2,64]{1,3,2,0:T(8,128)} %bitcast_dynamic-update-slice_fusion.2) | copy-start | bytes 786436
  131.7 24.6 %copy-start.4 = (bf16[4,128,2,64]{1,3,2,0:T(8,128)(2,1)S(1)}, bf16[4,128,2,64]{1,3,2,0:T(8,128)(2,1)}, u32[]{:S(2)}) copy-start(bf16[4,128,2,64]{1,3,2,0:T(8,128)(2,1)} %copy.99) | copy-start | bytes 393220
  131.7 24.6 %copy-start.11 = (pred[128,128]{1,0:T(8,128)(4,1)S(1)}, pred[128,128]{1,0:T(8,128)(4,1)}, u32[]{:S(2)}) copy-start(pred[128,128]{1,0:T(8,128)(4,1)} %iota_compare_fusion) | copy-start | bytes 49156
  131.7 25.3 %copy-start.10 = (bf16[512,128]{1,0:T(8,128)(2,1)S(1)}, bf16[512,128]{1,0:T(8,128)(2,1)}, u32[]{:S(2)}) copy-start(bf16[512,128]{1,0:T(8,128)(2,1)} %param.31) | copy-start | bytes 393220
  135.8 26.1 %all-to-all-start = ((bf16[4,128,384]{1,2,0:T(8,128)(2,1)}), bf16[4,128,384]{1,2,0:T(8,128)(2,1)S(1)}, u32[]{:S(2)}, u32[]{:S(2)}) async-start(bf16[4,128,384]{1,2,0:T(8,128)(2,1)} %copy_bitcast_fusion), calls=%async_computation | async-start | bytes 786432 | tf_op jit(solution)/shard_map/all_to_all | solution.py:162
  161.9 8.1 %all-to-all-start.1 = ((bf16[4,128,128]{1,2,0:T(8,128)(2,1)}), bf16[4,128,128]{1,2,0:T(8,128)(2,1)S(1)}, u32[]{:S(2)}, u32[]{:S(2)}) async-start(bf16[4,128,128]{1,2,0:T(8,128)(2,1)} %copy_bitcast_fusion.1), calls=%async_computation.1 | async-start | bytes 262144 | tf_op jit(solution)/shard_map/all_to_all | solution.py:163
  166.2 32.4 %all-gather.14.cloned.1.call-start = ((), (), s32[]{:S(2)}) async-start(), calls=%async_computation.5 | async-start | bytes 2621440 | tf_op jit(solution)/shard_map/all_gather | solution.py:174
  170.0 2.3 copy-start.5
  170.0 2.3 copy-start.14
  170.0 2.7 copy-start.15
  173.7 149.2 %all-gather.16.cloned.1.call-start = ((), (), s32[]{:S(2)}) async-start(), calls=%async_computation.6 | async-start | bytes 9437184 | tf_op jit(solution)/shard_map/all_gather | solution.py:178
  174.2 273.7 %all-gather.18.cloned.1.call-start = ((), (), s32[]{:S(2)}) async-start(), calls=%async_computation.7 | async-start | bytes 9437184 | tf_op jit(solution)/shard_map/all_gather | solution.py:185
  174.8 322.0 %copy-start.16 = (f32[2048]{0:T(1024)S(1)}, f32[2048]{0:T(1024)}, u32[]{:S(2)}) copy-start(f32[2048]{0:T(1024)} %param.41) | copy-start | bytes 24580
  174.8 320.8 %reduce-scatter.2.cloned.1.call-start = ((), (), s32[]{:S(2)}) async-start(), calls=%async_computation.8 | async-start | bytes 2621440 | tf_op jit(solution)/shard_map/reduce_scatter | solution.py:188
Sparse Core Ops, SparseCore 0:
  8.9 47.7 all-gather.9
  58.2 22.5 all-gather.11
  173.8 24.7 all-gather.13
  200.6 122.2 all-gather.15
  324.7 123.1 all-gather.17
  464.6 30.9 reduce-scatter.1
where the time goes:
time: 509 us; the launch traced here: 506 us
  waiting for transfers between devices  311 us (61%)
  blocking collectives  66.1 us (13%)
  other arithmetic  31.8 us (6%)
  matrix products  31.6 us (6%)
  local copies, waits for them, and re-layouts  26.1 us (5%)
  starting transfers between devices  24.1 us (5%)
  between operations  15.2 us (3%)
    all_gather x1, waiting for transfers between devices, local(): lax.all_gather(down_weight, 'sp', axis=1, tiled=True)  125 us
    all_gather x1, waiting for transfers between devices, local(): lax.all_gather(up_weight, 'sp', axis=0, tiled=True)  124 us
    all_gather x2, blocking collectives, prefix_2(): lax.all_gather(a.astype(kind), axis)  50.8 us
    reduce_scatter x1, waiting for transfers between devices, local(): lax.psum_scatter(partial_terms.astype(jnp.bfloat16), 'tp', scatter_dimens...  31.2 us
    all_gather x1, waiting for transfers between devices, local(): block_rows = lax.all_gather(normed, 'tp', axis=0, tiled=True)  23.7 us
    all_to_all x1, starting transfers between devices, local(): lax.all_to_all(wide_mixed, 'tp', split_axis=0, concat_axis=1, tiled=True)  19.7 us
    dot_general x1, matrix products, local(): jnp.dot(hidden, lax.all_gather(down_weight, 'sp', axis=1, tiled=True), pr...  16.5 us
    unnamed x1, blocking collectives  15.3 us
  transfers between devices with their start and end apart: 8, of which 5 were waited for; matrix products, arithmetic and copies ran while one was open for 13% of the time, Pallas kernels for 0%

commit v1 on v0

--- a/solution.py
+++ b/solution.py
@@ -1,7 +1,13 @@
+import functools
+
 import jax
 import jax.numpy as jnp
 from jax import lax
+from jax.experimental import pallas as pl
+from jax.experimental.pallas import tpu as pltpu
 from jax.sharding import PartitionSpec as P
+
+MESH = pl.DeviceIdType.MESH
 
 WIDE_DIM = 128
 NARROW_DIM = 64
@@ -11,26 +17,39 @@
 epsilon = 1e-06
 
 
-def prefix_2(array, axis, join, neutral):
-    place = lax.axis_index(axis)
-    gathered = jax.tree.map(
-        lambda a, kind: lax.all_gather(a.astype(kind), axis),
-        array,
-        (jnp.bfloat16, jnp.bfloat16, jnp.bfloat16, jnp.bfloat16),
-    )
-    state = jax.tree.map(lambda a, e: jnp.zeros_like(a) + jnp.asarray(e, a.dtype), array, neutral)
-
-    def one(turn, state):
-        return join(
-            state,
-            jax.tree.map(
-                lambda a, own: lax.dynamic_index_in_dim(a, turn, 0, False).astype(own.dtype),
-                gathered,
-                array,
-            ),
-        )
-
-    return lax.fori_loop(0, place, one, state)
+def pack_states(items):
+    wide_decay, wide_state, narrow_decay, narrow_state = items
+    decays = jnp.concatenate([wide_decay, narrow_decay])
+    decays = jnp.pad(decays[None, :], ((0, 15), (0, 128 - decays.shape[0])))
+    return jnp.concatenate(
+        [wide_state.reshape(-1, 128), narrow_state.reshape(-1, 128), decays], axis=0
+    ).astype(jnp.bfloat16)
+
+
+def unpack_states(packed, like):
+    packed = packed.astype(jnp.float32)
+    wide_rows, narrow_rows = like[1].size // 128, like[3].size // 128
+    decays = packed[wide_rows + narrow_rows]
+    wide_heads, narrow_heads = like[0].shape[0], like[2].shape[0]
+    return (
+        decays[:wide_heads],
+        packed[:wide_rows].reshape(like[1].shape),
+        decays[wide_heads : wide_heads + narrow_heads],
+        packed[wide_rows : wide_rows + narrow_rows].reshape(like[3].shape),
+    )
+
+
+def earlier_states(own, axis, count):
+    whole, before, distance = own, None, 1
+    while distance < count:
+        arrived = lax.ppermute(
+            pack_states(whole), axis, [(i, i + distance) for i in range(count - distance)]
+        )
+        arrived = unpack_states(arrived, own)
+        before = arrived if before is None else combine_states(arrived, before)
+        whole = combine_states(arrived, whole)
+        distance *= 2
+    return before
 
 
 def rotate(packed, head_dim, positions):
@@ -90,7 +109,7 @@
         return (carried * jnp.exp(decay_sum)[:, None, None] + contribution, carried)
 
     initial = jnp.zeros((count_of_heads, head_dim, head_dim), jnp.float32)
-    closing, before = lax.scan(advance, initial, (span_total, own_state))
+    closing, before = lax.scan(advance, initial, (span_total, own_state), unroll=True)
     device_decay = jnp.exp(jnp.sum(span_total, axis=0))
     return (queries, cumulative, within, span_total, before, closing, device_decay)
 
@@ -144,20 +163,31 @@
     narrow_parts = span_terms(
         narrow_query, narrow_key, narrow_value, narrow_decay, NARROW_DIM, offset
     )
-    identity = (
-        jnp.ones_like(wide_parts[6]),
-        jnp.zeros_like(wide_parts[5]),
-        jnp.ones_like(narrow_parts[6]),
-        jnp.zeros_like(narrow_parts[5]),
-    )
-    prefixes = prefix_2(
+    prefixes = earlier_states(
         (wide_parts[6], wide_parts[5], narrow_parts[6], narrow_parts[5]),
         "sp",
-        combine_states,
-        identity,
+        lax.axis_size("sp"),
     )
     wide_mixed = finish(wide_parts, prefixes[1], wide_gate, WIDE_DIM)
     narrow_mixed = finish(narrow_parts, prefixes[3], narrow_gate, NARROW_DIM)
+    columns = down_weight.shape[1]
+    count_sp, count_tp = lax.axis_size("sp"), lax.axis_size("tp")
+    if columns % 128 == 0 and count_sp % 2 == 0 and count_sp >= 4 and count_tp > 1:
+        up_whole = lax.all_gather(up_weight, "sp", axis=0, tiled=True)
+        return tail_call(
+            wide_mixed, narrow_mixed, wide_out, narrow_out, residual,
+            gain_mix, gain_pre, gain_mlp, up_whole, down_weight, count_sp, count_tp,
+        )
+    return tail_plain(
+        wide_mixed, narrow_mixed, wide_out, narrow_out, residual,
+        gain_mix, gain_pre, gain_mlp, up_weight, down_weight,
+    )
+
+
+def tail_plain(
+    wide_mixed, narrow_mixed, wide_out, narrow_out, residual,
+    gain_mix, gain_pre, gain_mlp, up_weight, down_weight,
+):
     wide_rows, narrow_rows = (
         lax.all_to_all(wide_mixed, "tp", split_axis=0, concat_axis=1, tiled=True),
         lax.all_to_all(narrow_mixed, "tp", split_axis=0, concat_axis=1, tiled=True),
@@ -191,6 +221,281 @@
     return (updated.astype(jnp.float32) + rms_scale(lowered, gain_mlp)).astype(jnp.bfloat16)
 
 
+PIECES = 2
+
+
+def tail_kernel(
+    count_sp, count_tp,
+    wide_mixed, narrow_mixed, wide_out, narrow_out, residual,
+    gain_mix, gain_pre, gain_mlp, up_hbm, down_hbm, result,
+    up_held, slots, part_out, part_in, rows, hidden, low_out, low_in, updated, lowered,
+    line_send, line_recv, pair_send, pair_recv, part_send, part_recv,
+    row_send, row_recv, low_send, low_recv, local_sem,
+):
+    line = count_sp // 2
+    sp, tp = lax.axis_index("sp"), lax.axis_index("tp")
+    a, b = sp // 2, lax.rem(sp, 2)
+    block_rows = residual.shape[0]
+    length, features = rows.shape
+    depth, columns = slots.shape[1], slots.shape[2]
+    piece = depth // PIECES
+
+    def at(line_place, pair_place):
+        return (line_place * 2 + pair_place, tp)
+
+    def peer(offset):
+        return (sp, lax.rem(tp + offset, count_tp))
+
+    own_down = pltpu.make_async_copy(down_hbm, slots.at[sp], local_sem.at[0])
+    own_down.start()
+    load_up = pltpu.make_async_copy(up_hbm, up_held, local_sem.at[1])
+    load_up.start()
+
+    barrier = pltpu.get_barrier_semaphore()
+    greeted = [at(lax.rem(a + 1, line), b), at(lax.rem(a + line - 1, line), b), at(a, 1 - b)]
+    greeted += [peer(offset) for offset in range(1, count_tp)]
+    for other in greeted:
+        pl.semaphore_signal(barrier, inc=1, device_id=other, device_id_type=MESH)
+    pl.semaphore_wait(barrier, len(greeted))
+    own_down.wait()
+
+    def chunk(place, index):
+        return slots.at[place, pl.ds(index * piece, piece)]
+
+    def right_copy(step, index, place):
+        ref = chunk(place * 2 + b, index)
+        return pltpu.make_async_remote_copy(
+            src_ref=ref, dst_ref=ref,
+            send_sem=line_send.at[0, step, index], recv_sem=line_recv.at[0, step, index],
+            device_id=at(jnp.minimum(a + 1, line - 1), b), device_id_type=MESH,
+        )
+
+    def left_copy(step, index, place):
+        ref = chunk(place * 2 + b, index)
+        return pltpu.make_async_remote_copy(
+            src_ref=ref, dst_ref=ref,
+            send_sem=line_send.at[1, step, index], recv_sem=line_recv.at[1, step, index],
+            device_id=at(jnp.maximum(a - 1, 0), b), device_id_type=MESH,
+        )
+
+    def pair_copy(index, place, column):
+        ref = chunk(place * 2 + column, index)
+        return pltpu.make_async_remote_copy(
+            src_ref=ref, dst_ref=ref,
+            send_sem=pair_send.at[place, index], recv_sem=pair_recv.at[place, index],
+            device_id=at(a, 1 - b), device_id_type=MESH,
+        )
+
+    for index in range(PIECES):
+        @pl.when(a + 1 < line)
+        def _():
+            right_copy(0, index, a).start()
+
+        @pl.when(a >= 1)
+        def _():
+            left_copy(0, index, a).start()
+
+        pair_copy(index, a, b).start()
+
+    def relay(step):
+        for index in range(PIECES):
+            @pl.when(a - 1 - step >= 0)
+            def _():
+                place = a - 1 - step
+                right_copy(step, index, place).wait_recv()
+
+                @pl.when(a + 1 < line)
+                def _():
+                    right_copy(step + 1, index, place).start()
+
+                pair_copy(index, place, b).start()
+
+            @pl.when(a + 1 + step < line)
+            def _():
+                place = a + 1 + step
+                left_copy(step, index, place).wait_recv()
+
+                @pl.when(a >= 1)
+                def _():
+                    left_copy(step + 1, index, place).start()
+
+                pair_copy(index, place, b).start()
+
+    def project(start):
+        taken = pl.ds(pl.multiple_of(start * block_rows, block_rows), block_rows)
+        return jnp.dot(
+            wide_mixed[taken, :], wide_out[...], preferred_element_type=jnp.float32
+        ) + jnp.dot(narrow_mixed[taken, :], narrow_out[...], preferred_element_type=jnp.float32)
+
+    def part_copy(offset):
+        return pltpu.make_async_remote_copy(
+            src_ref=part_out.at[offset], dst_ref=part_in.at[offset],
+            send_sem=part_send.at[offset], recv_sem=part_recv.at[offset],
+            device_id=peer(offset), device_id_type=MESH,
+        )
+
+    @pl.loop(1, count_tp)
+    def _(offset):
+        part_out[offset] = project(lax.rem(tp + offset, count_tp)).astype(jnp.bfloat16)
+        part_copy(offset).start()
+
+    lowered[...] = project(tp)
+    for offset in range(1, count_tp):
+        part_copy(offset).wait_recv()
+        lowered[...] += part_in[offset].astype(jnp.float32)
+
+    mine = pl.ds(pl.multiple_of(tp * block_rows, block_rows), block_rows)
+    moved = residual[...].astype(jnp.float32) + rms_scale(lowered[...], gain_mix[...])
+    moved = moved.astype(jnp.bfloat16)
+    updated[...] = moved
+    rows[mine, :] = rms_scale(moved.astype(jnp.float32), gain_pre[...]).astype(jnp.bfloat16)
+
+    def row_copy(offset):
+        return pltpu.make_async_remote_copy(
+            src_ref=rows.at[mine], dst_ref=rows.at[mine],
+            send_sem=row_send.at[offset], recv_sem=row_recv.at[offset],
+            device_id=peer(offset), device_id_type=MESH,
+        )
+
+    for offset in range(1, count_tp):
+        row_copy(offset).start()
+    relay(0)
+    load_up.wait()
+    for offset in range(1, count_tp):
+        row_copy(offset).wait_recv()
+
+    width = 256
+
+    @pl.loop(0, hidden.shape[1] // width)
+    def _(tile):
+        taken = pl.ds(pl.multiple_of(tile * width, width), width)
+        rectified = jax.nn.relu(
+            jnp.dot(rows[...], up_held[:, taken], preferred_element_type=jnp.float32)
+        )
+        hidden[:, taken] = (rectified * rectified).astype(jnp.bfloat16)
+
+    def low_copy(offset, block):
+        start = lax.rem(tp + offset, count_tp) * block_rows
+        return pltpu.make_async_remote_copy(
+            src_ref=low_out.at[block, pl.ds(pl.multiple_of(start, block_rows), block_rows)],
+            dst_ref=low_in.at[offset, block],
+            send_sem=low_send.at[offset, block], recv_sem=low_recv.at[offset, block],
+            device_id=peer(offset), device_id_type=MESH,
+        )
+
+    def consume(block):
+        low_out[block] = jnp.dot(
+            hidden[...], slots[block], preferred_element_type=jnp.float32
+        ).astype(jnp.bfloat16)
+        for offset in range(1, count_tp):
+            low_copy(offset, block).start()
+
+    def at_distance(act, distance):
+        @pl.when(a - distance >= 0)
+        def _():
+            act(a - distance)
+
+        @pl.when((a + distance < line) & (distance > 0))
+        def _():
+            act(a + distance)
+
+    def from_pair(place):
+        for index in range(PIECES):
+            pair_copy(index, place, 1 - b).wait_recv()
+        consume(place * 2 + 1 - b)
+
+    @pl.loop(0, line)
+    def _(distance):
+        @pl.when(distance + 1 <= line - 2)
+        def _():
+            relay(distance + 1)
+
+        at_distance(lambda place: consume(place * 2 + b), distance)
+        at_distance(from_pair, distance)
+
+    for block in range(count_sp):
+        taken = slice(block * columns, (block + 1) * columns)
+        total = low_out[block, mine, :].astype(jnp.float32)
+        for offset in range(1, count_tp):
+            low_copy(offset, block).wait_recv()
+            total += low_in[offset, block].astype(jnp.float32)
+        lowered[:, taken] = total
+    result[...] = (
+        updated[...].astype(jnp.float32) + rms_scale(lowered[...], gain_mlp[...])
+    ).astype(jnp.bfloat16)
+
+    for offset in range(1, count_tp):
+        part_copy(offset).wait_send()
+        row_copy(offset).wait_send()
+
+        @pl.loop(0, count_sp)
+        def _(block):
+            low_copy(offset, block).wait_send()
+
+    for index in range(PIECES):
+        @pl.loop(0, line)
+        def _(place):
+            pair_copy(index, place, b).wait_send()
+
+        @pl.loop(0, line - 1)
+        def _(step):
+            @pl.when((a + 1 < line) & (a - step >= 0))
+            def _():
+                right_copy(step, index, jnp.maximum(a - step, 0)).wait_send()
+
+            @pl.when((a >= 1) & (a + step < line))
+            def _():
+                left_copy(step, index, jnp.minimum(a + step, line - 1)).wait_send()
+
+
+def tail_call(
+    wide_mixed, narrow_mixed, wide_out, narrow_out, residual,
+    gain_mix, gain_pre, gain_mlp, up_whole, down_weight, count_sp, count_tp,
+):
+    block_rows, features = residual.shape
+    length = block_rows * count_tp
+    depth, columns = down_weight.shape
+    half, line = jnp.bfloat16, count_sp // 2
+    dma = pltpu.SemaphoreType.DMA
+    vmem = pl.BlockSpec(memory_space=pltpu.VMEM)
+    anywhere = pl.BlockSpec(memory_space=pl.ANY)
+    return pl.pallas_call(
+        functools.partial(tail_kernel, count_sp, count_tp),
+        out_shape=jax.ShapeDtypeStruct(residual.shape, half),
+        in_specs=[vmem] * 8 + [anywhere] * 2,
+        out_specs=vmem,
+        scratch_shapes=[
+            pltpu.VMEM(up_whole.shape, half),
+            pltpu.VMEM((count_sp, depth, columns), half),
+            pltpu.VMEM((count_tp, block_rows, features), half),
+            pltpu.VMEM((count_tp, block_rows, features), half),
+            pltpu.VMEM((length, features), half),
+            pltpu.VMEM((length, depth), half),
+            pltpu.VMEM((count_sp, length, columns), half),
+            pltpu.VMEM((count_tp, count_sp, block_rows, columns), half),
+            pltpu.VMEM((block_rows, features), half),
+            pltpu.VMEM((block_rows, features), jnp.float32),
+            dma((2, line - 1, PIECES)),
+            dma((2, line - 1, PIECES)),
+            dma((line, PIECES)),
+            dma((line, PIECES)),
+            dma((count_tp,)),
+            dma((count_tp,)),
+            dma((count_tp,)),
+            dma((count_tp,)),
+            dma((count_tp, count_sp)),
+            dma((count_tp, count_sp)),
+            dma((2,)),
+        ],
+        compiler_params=pltpu.CompilerParams(
+            collective_id=0, has_side_effects=True, vmem_limit_bytes=52 * 1024 * 1024
+        ),
+    )(
+        wide_mixed, narrow_mixed, wide_out, narrow_out, residual,
+        gain_mix[None, :], gain_pre[None, :], gain_mlp[None, :], up_whole, down_weight,
+    )
+
+
 def solution(mesh):
     return jax.shard_map(
         local,

time: 509 us -> 252 us (0.50)
  waiting for transfers between devices: 311 us -> 58.3 us
  Pallas kernels: 0 us -> 102 us
  blocking collectives: 66.1 us -> 0 us
  matrix products: 31.6 us -> 11.5 us
  starting transfers between devices: 24.1 us -> 5.88 us
  other arithmetic: 31.8 us -> 24.8 us
  local copies, waits for them, and re-layouts: 26.1 us -> 31.7 us
    all_gather x5 -> x1, waiting for transfers between devices: 273 us -> 39.8 us  [local(): up_whole = lax.all_gather(up_weight, 'sp', axis=0, tiled=True)]
    pallas_call x0 -> x1, Pallas kernels: none -> 102 us  [tail_call(): pl.pallas_call(functools.partial(tail_kernel, count_sp, count_tp), out_sh...]
    all_gather x2 -> x0, blocking collectives: 50.8 us -> none  [prefix_2(): lax.all_gather(a.astype(kind), axis)]
    reduce_scatter x1 -> x0, waiting for transfers between devices: 31.2 us -> none  [local(): lax.psum_scatter(partial_terms.astype(jnp.bfloat16), 'tp', scatter_dimens...]
    all_to_all x2 -> x0, starting transfers between devices: 24 us -> none  [the longest x1 19.7 us: local(): lax.all_to_all(wide_mixed, 'tp', split_axis=0, concat_axis=1, tiled=True)]
    dot_general x3 -> x0, matrix products: 22.5 us -> none  [the longest x1 16.5 us: local(): jnp.dot(hidden, lax.all_gather(down_weight, 'sp', axis=1, tiled=True), pr...]
    ppermute x0 -> x3, waiting for transfers between devices: none -> 17.8 us  [earlier_states(): lax.ppermute(pack_states(whole), axis, [(i, i + distance) for i in range(...]
    unnamed x1 -> x0, blocking collectives: 15.3 us -> none
  transfers between devices with their start and end apart: 8 -> 4, of which waited for: 5 -> 4; matrix products, arithmetic and copies ran while one was open for 13% -> 27% of each run, Pallas kernels for 0% -> 0%
where the time goes in v1:
time: 252 us; the launch traced here: 248 us
  Pallas kernels  102 us (40%)
  waiting for transfers between devices  58.3 us (23%)
  local copies, waits for them, and re-layouts  31.7 us (13%)
  other arithmetic  24.8 us (10%)
  between operations  13.9 us (6%)
  matrix products  11.5 us (5%)
  starting transfers between devices  5.88 us (2%)
    pallas_call x1, Pallas kernels, tail_call(): pl.pallas_call(functools.partial(tail_kernel, count_sp, count_tp), out_sh...  102 us
    all_gather x1, waiting for transfers between devices, local(): up_whole = lax.all_gather(up_weight, 'sp', axis=0, tiled=True)  39.8 us
    ppermute x3, waiting for transfers between devices, earlier_states(): lax.ppermute(pack_states(whole), axis, [(i, i + distance) for i in range(...  17.8 us
    unnamed x39, local copies, waits for them, and re-layouts  6.68 us
    another operation x9, other arithmetic  5.95 us
    ppermute x3, starting transfers between devices, earlier_states(): lax.ppermute(pack_states(whole), axis, [(i, i + distance) for i in range(...  5.87 us
  transfers between devices with their start and end apart: 4, of which 4 were waited for; matrix products, arithmetic and copies ran while one was open for 27% of the time, Pallas kernels for 0%

profile of v1, /device:TPU:25, one launch (start us, length us, event | category | flops | bytes accessed | tf_op | source)
XLA Modules:
  0.0 247.6 jit_solution(13253830822580383880)
XLA Ops:
  6.5 0.7 all-gather.2.cloned.1.call-update
  7.3 0.8 copy.120
  9.1 1.2 copy.77
  10.4 1.2 copy.80
  12.2 1.1 subtract_convert_fusion
  14.3 1.0 copy.92
  15.3 0.7 convert.86
  16.1 1.0 copy.105
  17.1 0.7 convert.87
  17.8 0.8 copy.121
  20.2 0.7 copy.96
  20.9 0.8 fusion.98
  21.6 0.7 copy.97
  23.5 1.8 fusion.62
  25.4 0.9 fusion.50
  26.3 0.8 multiply_add_fusion.4
  27.1 0.7 squeeze.40
  28.0 0.7 mul.602
  28.7 0.7 mul.618
  29.5 0.6 mul.621
  30.2 0.7 mul.624
  31.0 0.7 mul.625
  31.7 1.1 fusion.101
  32.8 1.2 fusion.102
  34.2 1.4 fusion.97
  35.7 0.8 fusion.20
  36.5 0.9 multiply_add_fusion.1
  37.7 0.6 fusion.58
  38.3 3.1 %collective-permute-start = (bf16[464,128]{1,0:T(8,128)(2,1)}, bf16[464,128]{1,0:T(8,128)(2,1)S(1)}, u32[]{:S(2)}, u32[]{:S(2)}) collective-permute-start(bf16[464,128]{1,0:T(8,128)(2,1)} %fusion.58), channel_id=1, source_target_pairs={{0,4},{4,8},{8,12},{12,16},{16,20},{20,24},{24,28},{1,5},{5,9},{9,... | collective-permute-start | bytes 356360 | tf_op jit(solution)/shard_map/ppermute | solution.py:45
  42.3 0.9 bitcast_dynamic-update-slice_fusion.3
  43.1 0.9 bitcast_dynamic-update-slice_fusion.2
  44.0 0.7 broadcast_bitcast_fusion.1
  44.7 1.3 mul.631
  46.0 0.9 mul.632
  47.1 0.7 copy.108
  47.9 1.0 concatenate.64
  49.2 1.0 concatenate.65
  50.2 1.0 copy.79
  51.3 0.6 iota_compare_fusion.1
  52.1 0.6 fusion.92
  52.7 0.7 fusion.94
  53.5 0.8 fusion.91
  54.4 1.3 collective-permute-start.1
  55.9 0.7 reshape.497
  56.6 0.7 slice.206
  57.4 2.6 %collective-permute-done.1 = bf16[464,128]{1,0:T(8,128)(2,1)S(1)} collective-permute-done((bf16[464,128]{1,0:T(8,128)(2,1)S(1)}, bf16[464,128]{1,0:T(8,128)(2,1)S(1)}, u32[]{:S(2)}, u32[]{:S(2)}) %collective-permute-start.1) | collective-permute-done | bytes 118816 | tf_op jit(solution)/shard_map/ppermute | solution.py:45
  60.7 0.8 add_convert_fusion.3
  61.7 1.5 collective-permute-start.2
  63.3 15.1 %collective-permute-done.2 = bf16[464,128]{1,0:T(8,128)(2,1)S(1)} collective-permute-done((bf16[464,128]{1,0:T(8,128)(2,1)S(1)}, bf16[464,128]{1,0:T(8,128)(2,1)S(1)}, u32[]{:S(2)}, u32[]{:S(2)}) %collective-permute-start.2) | collective-permute-done | bytes 118816 | tf_op jit(solution)/shard_map/ppermute | solution.py:45
  78.5 0.9 add_add_fusion.1
  79.4 2.1 fusion.7
  81.5 1.7 multiply_reduce_fusion.1
  83.8 0.7 mul.689
  84.5 1.8 copy.116
  86.3 0.9 slice.214
  87.2 1.0 add_add_fusion
  88.3 2.8 %fusion = f32[4,128,3,128]{1,3,2,0:T(8,128)} fusion(f32[1,3,128,128]{3,2,1,0:T(8,128)} %get-tuple-element.16, f32[1,3,128,128]{3,2,1,0:T(8,128)} %get-tuple-element.17, f32[1,3,128,128]{3,2,1,0:T(8,128)} %get-tuple-element.18, f32[4]{0:T(128)} %copy-done.15, f32[4,128,3]{1,2,0:T(4,128)S(1)} %copy.101, f32[4,3]{1,0:T(4,128)} %subtract_exponential_fusion, ...), kind=kOutput, calls=%fused_computation.2 | convolution fusion | flops 52494336 | bytes 1972288 | tf_op jit(solution)/shard_map/nihd,nhde->nihe/dot_general | solution.py:123
  91.1 3.2 %multiply_reduce_fusion = (f32[4,128,3]{1,2,0:T(4,128)S(1)}, f32[4,128,3,128]{1,3,2,0:T(8,128)}) fusion(f32[4,128,3,128]{1,3,2,0:T(8,128)} %fusion, bf16[4,128,3,128]{3,2,1,0:T(4,128)(2,1)S(1)} %reshape.510, f32[4,3,128]{2,1,0:T(4,128)S(1)} %copy.84, pred[128,128]{1,0:T(8,128)(4,1)} %iota_compare_fusion.1, f32[4,128,3,64]{3,1,2,0:T(8,128)S(1)} %copy.82, ...), kind=kOutput, calls=%fused_computation.23 | convolution fusion | flops 103414272 | bytes 3174400 | tf_op jit(solution)/shard_map/nhij,njhd->nihd/dot_general | solution.py:98
  94.7 1.5 copy.122
  96.3 1.1 fusion.42.narrow_mixed
  97.4 1.2 fusion.16.wide_mixed
  98.6 39.8 %all-gather.2.cloned.1.call-done.up_hbm = bf16[2048,2048]{1,0:T(8,128)(2,1)} async-done(((bf16[256,2048]{1,0:T(8,128)(2,1)}), bf16[2048,2048]{1,0:T(8,128)(2,1)}) %all-gather.2.cloned.1.call-update) | async-done | bytes 8388624 | tf_op jit(solution)/shard_map/all_gather | solution.py:176
  138.4 101.6 %shard_map.172 = bf16[128,2048]{1,0:T(8,128)(2,1)S(1)} custom-call(bf16[512,384]{1,0:T(8,128)(2,1)S(1)} %fusion.16.wide_mixed, bf16[512,128]{1,0:T(8,128)(2,1)S(1)} %fusion.42.narrow_mixed, bf16[384,2048]{1,0:T(8,128)(2,1)} %wide_out.1, bf16[128,2048]{1,0:T(8,128)(2,1)S(1)} %copy-done, bf16[128,2048]{1,0:T(8,128)(2,1)} %residual.1, f32[1,2048]{1,0:T(1,128)S(1)} %bitcast.175, ...), custom_call_target="tpu_custom_call" | custom-call | tf_op jit(solution)/shard_map/pallas_call | solution.py:462
  240.0 0.8 copy.151
  (106 shorter events, 10.6 us)
Async XLA Ops:
  6.5 7.6 %copy-start.7 = (bf16[512,384]{1,0:T(8,128)(2,1)S(1)}, bf16[512,384]{1,0:T(8,128)(2,1)}, u32[]{:S(2)}) copy-start(bf16[512,384]{1,0:T(8,128)(2,1)} %param.20) | copy-start | bytes 1179652
  6.5 131.8 %all-gather.2.cloned.1.call-start = ((), (), s32[]{:S(2)}) async-start(), calls=%async_computation | async-start | bytes 9437184 | tf_op jit(solution)/shard_map/all_gather | solution.py:176
  8.1 14.2 %copy-start.8 = (bf16[512,128]{1,0:T(8,128)(2,1)S(1)}, bf16[512,128]{1,0:T(8,128)(2,1)}, u32[]{:S(2)}) copy-start(bf16[512,128]{1,0:T(8,128)(2,1)} %param.24) | copy-start | bytes 393220
  19.6 0.6 copy-start.10
  22.6 15.1 %copy-start.5 = (bf16[4,128,2,64]{1,3,2,0:T(8,128)(2,1)}, bf16[4,128,2,64]{1,3,2,0:T(8,128)(2,1)S(1)}, u32[]{:S(2)}) copy-start(bf16[4,128,2,64]{1,3,2,0:T(8,128)(2,1)S(1)} %copy.99) | copy-start | bytes 393220
  23.2 3.9 %copy-start.12 = (f32[2]{0:T(128)}, f32[2]{0:T(128)S(1)}, u32[]{:S(2)}) copy-start(f32[2]{0:T(128)S(1)} %get-tuple-element.45) | copy-start | bytes 28
  23.2 3.9 %copy-start.13 = (f32[2]{0:T(128)}, f32[2]{0:T(128)S(1)}, u32[]{:S(2)}) copy-start(f32[2]{0:T(128)S(1)} %get-tuple-element.46) | copy-start | bytes 28
  23.2 3.9 %copy-start.14 = (f32[2]{0:T(128)}, f32[2]{0:T(128)S(1)}, u32[]{:S(2)}) copy-start(f32[2]{0:T(128)S(1)} %get-tuple-element.43) | copy-start | bytes 28
  23.5 17.9 %copy-start.11 = (f32[4,1,2]{0,2,1:T(2,128)S(1)}, f32[4,1,2]{0,2,1:T(2,128)}, u32[]{:S(2)}) copy-start(f32[4,1,2]{0,2,1:T(2,128)} %copy-done.10) | copy-start | bytes 100
  25.4 1.7 copy-start.4
  38.3 13.7 %collective-permute-start = (bf16[464,128]{1,0:T(8,128)(2,1)}, bf16[464,128]{1,0:T(8,128)(2,1)S(1)}, u32[]{:S(2)}, u32[]{:S(2)}) collective-permute-start(bf16[464,128]{1,0:T(8,128)(2,1)} %fusion.58), channel_id=1, source_target_pairs={{0,4},{4,8},{8,12},{12,16},{16,20},{20,24},{24,28},{1,5},{5,9},{9,... | collective-permute-start | bytes 356360 | tf_op jit(solution)/shard_map/ppermute | solution.py:45
  44.0 0.7 copy-start.9
  51.3 28.2 %copy-start.15 = (f32[4]{0:T(128)}, f32[4]{0:T(128)S(1)}, u32[]{:S(2)}) copy-start(f32[4]{0:T(128)S(1)} %pad.20.clone) | copy-start | bytes 52
  54.4 5.6 %collective-permute-start.1 = (bf16[464,128]{1,0:T(8,128)(2,1)S(1)}, bf16[464,128]{1,0:T(8,128)(2,1)S(1)}, u32[]{:S(2)}, u32[]{:S(2)}) collective-permute-start(bf16[464,128]{1,0:T(8,128)(2,1)S(1)} %fusion.59), channel_id=1, source_target_pairs={{0,8},{4,12},{8,16},{12,20},{16,24},{20,28},{1,9},{5,13},{9,17},{1... | collective-permute-start | bytes 356360 | tf_op jit(solution)/shard_map/ppermute | solution.py:45
  61.7 16.7 %collective-permute-start.2 = (bf16[464,128]{1,0:T(8,128)(2,1)S(1)}, bf16[464,128]{1,0:T(8,128)(2,1)S(1)}, u32[]{:S(2)}, u32[]{:S(2)}) collective-permute-start(bf16[464,128]{1,0:T(8,128)(2,1)S(1)} %fusion.60), channel_id=1, source_target_pairs={{0,16},{4,20},{8,24},{12,28},{1,17},{5,21},{9,25},{13,29},{2,18},{... | collective-permute-start | bytes 356360 | tf_op jit(solution)/shard_map/ppermute | solution.py:45
  78.4 4.7 %copy-start.6 = (bf16[464,128]{1,0:T(8,128)(2,1)}, bf16[464,128]{1,0:T(8,128)(2,1)S(1)}, u32[]{:S(2)}) copy-start(bf16[464,128]{1,0:T(8,128)(2,1)S(1)} %collective-permute-done.2) | copy-start | bytes 356356
  83.7 54.6 %copy-start = (bf16[128,2048]{1,0:T(8,128)(2,1)S(1)}, bf16[128,2048]{1,0:T(8,128)(2,1)}, u32[]{:S(2)}) copy-start(bf16[128,2048]{1,0:T(8,128)(2,1)} %narrow_out.1) | copy-start | bytes 1572868
  83.7 54.6 %copy-start.1 = (f32[2048]{0:T(1024)S(1)}, f32[2048]{0:T(1024)}, u32[]{:S(2)}) copy-start(f32[2048]{0:T(1024)} %param.33) | copy-start | bytes 24580
  83.8 54.6 %copy-start.2 = (f32[2048]{0:T(1024)S(1)}, f32[2048]{0:T(1024)}, u32[]{:S(2)}) copy-start(f32[2048]{0:T(1024)} %param.34) | copy-start | bytes 24580
  83.8 54.6 %copy-start.3 = (f32[2048]{0:T(1024)S(1)}, f32[2048]{0:T(1024)}, u32[]{:S(2)}) copy-start(f32[2048]{0:T(1024)} %param.35) | copy-start | bytes 24580
Sparse Core Ops, SparseCore 0:
  9.5 128.8 all-gather.1

commit v2 on v1

--- a/solution.py
+++ b/solution.py
@@ -157,6 +157,18 @@
     gain_pre,
     gain_mlp,
 ):
+    columns = down_weight.shape[1]
+    count_sp, count_tp = lax.axis_size("sp"), lax.axis_size("tp")
+    if (
+        columns % 128 == 0 and count_sp % 4 == 0 and count_sp >= 8 and count_tp > 1
+        and narrow_query.shape[1] % 128 == 0
+    ):
+        return whole_call(
+            (wide_query, wide_key, wide_value, wide_gate),
+            (narrow_query, narrow_key, narrow_value, narrow_gate),
+            wide_decay, narrow_decay, residual, wide_out, narrow_out,
+            up_weight, down_weight, gain_mix, gain_pre, gain_mlp, count_sp, count_tp,
+        )
     length = wide_query.shape[0]
     offset = lax.axis_index("sp") * length
     wide_parts = span_terms(wide_query, wide_key, wide_value, wide_decay, WIDE_DIM, offset)
@@ -170,14 +182,6 @@
     )
     wide_mixed = finish(wide_parts, prefixes[1], wide_gate, WIDE_DIM)
     narrow_mixed = finish(narrow_parts, prefixes[3], narrow_gate, NARROW_DIM)
-    columns = down_weight.shape[1]
-    count_sp, count_tp = lax.axis_size("sp"), lax.axis_size("tp")
-    if columns % 128 == 0 and count_sp % 2 == 0 and count_sp >= 4 and count_tp > 1:
-        up_whole = lax.all_gather(up_weight, "sp", axis=0, tiled=True)
-        return tail_call(
-            wide_mixed, narrow_mixed, wide_out, narrow_out, residual,
-            gain_mix, gain_pre, gain_mlp, up_whole, down_weight, count_sp, count_tp,
-        )
     return tail_plain(
         wide_mixed, narrow_mixed, wide_out, narrow_out, residual,
         gain_mix, gain_pre, gain_mlp, up_weight, down_weight,
@@ -224,21 +228,46 @@
 PIECES = 2
 
 
-def tail_kernel(
-    count_sp, count_tp,
-    wide_mixed, narrow_mixed, wide_out, narrow_out, residual,
-    gain_mix, gain_pre, gain_mlp, up_hbm, down_hbm, result,
-    up_held, slots, part_out, part_in, rows, hidden, low_out, low_in, updated, lowered,
-    line_send, line_recv, pair_send, pair_recv, part_send, part_recv,
-    row_send, row_recv, low_send, low_recv, local_sem,
+def swap_halves(values, head_dim):
+    half = head_dim // 2
+    if head_dim == 128:
+        return pltpu.roll(values, half, 1)
+    lane = lax.broadcasted_iota(jnp.int32, values.shape, 1)
+    return jnp.where(
+        lax.rem(lane, head_dim) < half,
+        pltpu.roll(values, 128 - half, 1),
+        pltpu.roll(values, half, 1),
+    )
+
+
+def whole_kernel(
+    count_sp, count_tp, wide_groups, narrow_groups,
+    wide_query, wide_key, wide_value, wide_gate,
+    narrow_query, narrow_key, narrow_value, narrow_gate,
+    tables, cum_rows, cum_lanes, total_lanes, earlier_lanes, device_lanes,
+    residual, wide_out, narrow_out, gain_mix, gain_pre, gain_mlp, up_hbm, down_hbm,
+    result,
+    up_slots, down_slots, part_out, part_in, rows, hidden, low_out, low_in, updated, lowered,
+    turned, within, carried, mixed, state, prefix, prefix_decay, state_out, state_in,
+    decay_out, decay_in,
+    line_send, line_recv, pair_send, pair_recv, swap_send, swap_recv, part_send, part_recv,
+    row_send, row_recv, low_send, low_recv, state_send, state_recv, decay_send, decay_recv,
+    local_sem,
 ):
     line = count_sp // 2
+    groups = wide_groups + narrow_groups
     sp, tp = lax.axis_index("sp"), lax.axis_index("tp")
     a, b = sp // 2, lax.rem(sp, 2)
+    twin = a + 1 - 2 * lax.rem(a, 2)
     block_rows = residual.shape[0]
     length, features = rows.shape
-    depth, columns = slots.shape[1], slots.shape[2]
-    piece = depth // PIECES
+    slots = (up_slots, down_slots)
+    depth, columns = down_slots.shape[1], down_slots.shape[2]
+    slab = up_slots.shape[1]
+    half = jnp.bfloat16
+    distances = []
+    while 2 ** len(distances) < count_sp:
+        distances.append(2 ** len(distances))
 
     def at(line_place, pair_place):
         return (line_place * 2 + pair_place, tp)
@@ -246,121 +275,301 @@
     def peer(offset):
         return (sp, lax.rem(tp + offset, count_tp))
 
-    own_down = pltpu.make_async_copy(down_hbm, slots.at[sp], local_sem.at[0])
+    own_up = pltpu.make_async_copy(up_hbm, up_slots.at[sp], local_sem.at[0])
+    own_up.start()
+    own_down = pltpu.make_async_copy(down_hbm, down_slots.at[sp], local_sem.at[1])
     own_down.start()
-    load_up = pltpu.make_async_copy(up_hbm, up_held, local_sem.at[1])
-    load_up.start()
 
     barrier = pltpu.get_barrier_semaphore()
-    greeted = [at(lax.rem(a + 1, line), b), at(lax.rem(a + line - 1, line), b), at(a, 1 - b)]
+    greeted = [at(a, 1 - b)]
+    greeted += [(lax.rem(sp + step, count_sp), tp) for step in distances]
+    greeted += [(lax.rem(sp + count_sp - step, count_sp), tp) for step in distances]
     greeted += [peer(offset) for offset in range(1, count_tp)]
     for other in greeted:
         pl.semaphore_signal(barrier, inc=1, device_id=other, device_id_type=MESH)
     pl.semaphore_wait(barrier, len(greeted))
+    own_up.wait()
     own_down.wait()
 
-    def chunk(place, index):
-        return slots.at[place, pl.ds(index * piece, piece)]
-
-    def right_copy(step, index, place):
-        ref = chunk(place * 2 + b, index)
+    def chunk(which, place, index):
+        piece = slots[which].shape[1] // PIECES
+        return slots[which].at[place, pl.ds(index * piece, piece)]
+
+    def remote(source, target, send, recv, device):
         return pltpu.make_async_remote_copy(
-            src_ref=ref, dst_ref=ref,
-            send_sem=line_send.at[0, step, index], recv_sem=line_recv.at[0, step, index],
-            device_id=at(jnp.minimum(a + 1, line - 1), b), device_id_type=MESH,
-        )
-
-    def left_copy(step, index, place):
-        ref = chunk(place * 2 + b, index)
-        return pltpu.make_async_remote_copy(
-            src_ref=ref, dst_ref=ref,
-            send_sem=line_send.at[1, step, index], recv_sem=line_recv.at[1, step, index],
-            device_id=at(jnp.maximum(a - 1, 0), b), device_id_type=MESH,
-        )
-
-    def pair_copy(index, place, column):
-        ref = chunk(place * 2 + column, index)
-        return pltpu.make_async_remote_copy(
-            src_ref=ref, dst_ref=ref,
-            send_sem=pair_send.at[place, index], recv_sem=pair_recv.at[place, index],
-            device_id=at(a, 1 - b), device_id_type=MESH,
-        )
-
-    for index in range(PIECES):
-        @pl.when(a + 1 < line)
-        def _():
-            right_copy(0, index, a).start()
-
-        @pl.when(a >= 1)
-        def _():
-            left_copy(0, index, a).start()
-
-        pair_copy(index, a, b).start()
-
-    def relay(step):
+            src_ref=source, dst_ref=target, send_sem=send, recv_sem=recv,
+            device_id=device, device_id_type=MESH,
+        )
+
+    def right_copy(which, step, index, place):
+        ref = chunk(which, place * 2 + b, index)
+        return remote(
+            ref, ref, line_send.at[which, 0, step, index], line_recv.at[which, 0, step, index],
+            at(jnp.minimum(a + 1, line - 1), b),
+        )
+
+    def left_copy(which, step, index, place):
+        ref = chunk(which, place * 2 + b, index)
+        return remote(
+            ref, ref, line_send.at[which, 1, step, index], line_recv.at[which, 1, step, index],
+            at(jnp.maximum(a - 1, 0), b),
+        )
+
+    def pair_copy(which, index, place, column):
+        ref = chunk(which, place * 2 + column, index)
+        return remote(
+            ref, ref, pair_send.at[which, place, index], pair_recv.at[which, place, index],
+            at(a, 1 - b),
+        )
+
+    def swap_copy(which, place):
+        ref = chunk(which, place * 2 + 1 - b, 1)
+        return remote(ref, ref, swap_send.at[which], swap_recv.at[which], at(twin, b))
+
+    def begin(which):
+        for index in range(PIECES):
+            @pl.when(a + 1 < line)
+            def _():
+                right_copy(which, 0, index, a).start()
+
+            @pl.when(a >= 1)
+            def _():
+                left_copy(which, 0, index, a).start()
+
+            pair_copy(which, index, a, b).start()
+
+    def to_pair(which, index, place):
+        if index == 0:
+            pair_copy(which, index, place, b).start()
+        else:
+            @pl.when(place != twin)
+            def _():
+                pair_copy(which, index, place, b).start()
+
+    def relay(which, step, first):
         for index in range(PIECES):
             @pl.when(a - 1 - step >= 0)
             def _():
                 place = a - 1 - step
-                right_copy(step, index, place).wait_recv()
-
-                @pl.when(a + 1 < line)
+                right_copy(which, step, index, place).wait_recv()
+
+                @pl.when((a + 1 < line) & (step < line - 2))
                 def _():
-                    right_copy(step + 1, index, place).start()
-
-                pair_copy(index, place, b).start()
+                    right_copy(which, jnp.minimum(step + 1, line - 2), index, place).start()
+
+                to_pair(which, index, place)
 
             @pl.when(a + 1 + step < line)
             def _():
                 place = a + 1 + step
-                left_copy(step, index, place).wait_recv()
-
-                @pl.when(a >= 1)
+                left_copy(which, step, index, place).wait_recv()
+
+                @pl.when((a >= 1) & (step < line - 2))
                 def _():
-                    left_copy(step + 1, index, place).start()
-
-                pair_copy(index, place, b).start()
+                    left_copy(which, jnp.minimum(step + 1, line - 2), index, place).start()
+
+                to_pair(which, index, place)
+
+        if first:
+            pair_copy(which, 1, a, 1 - b).wait_recv()
+            swap_copy(which, a).start()
+
+    def wait_pair(which, place):
+        pair_copy(which, 0, place, 1 - b).wait_recv()
+
+        @pl.when((place != a) & (place != twin))
+        def _():
+            pair_copy(which, 1, place, 1 - b).wait_recv()
+
+        @pl.when(place == twin)
+        def _():
+            swap_copy(which, place).wait_recv()
+
+    begin(0)
+
+    lane = lax.broadcasted_iota(jnp.int32, (SPAN, 128), 1)
+    position = lax.broadcasted_iota(jnp.int32, (SPAN, 128), 0)
+    causal = position >= lane
+    low_half = lane < 64
+    same_head = low_half == (position < 64)
+    plans = [(g, False, g) for g in range(wide_groups)]
+    plans += [(wide_groups + g, True, g) for g in range(narrow_groups)]
+
+    def dot(left, right, left_dim, right_dim):
+        return lax.dot_general(
+            left, right, (((left_dim,), (right_dim,)), ((), ())),
+            preferred_element_type=jnp.float32,
+        )
+
+    for g in range(groups):
+        state[g] = jnp.zeros((128, 128), jnp.float32)
+
+    @pl.loop(0, length // SPAN)
+    def _(span):
+        taken = pl.ds(pl.multiple_of(span * SPAN, SPAN), SPAN)
+        for g, narrow, own in plans:
+            lanes, mine = slice(g * 128, (g + 1) * 128), slice(own * 128, (own + 1) * 128)
+            if narrow:
+                query, key, value = narrow_query, narrow_key, narrow_value
+                head_dim, cosine, sine = NARROW_DIM, tables[2, taken, :], tables[3, taken, :]
+            else:
+                query, key, value = wide_query, wide_key, wide_value
+                head_dim, cosine, sine = WIDE_DIM, tables[0, taken, :], tables[1, taken, :]
+            raw = query[taken, mine].astype(jnp.float32)
+            spun = (raw * cosine + swap_halves(raw, head_dim) * sine).astype(half)
+            turned[taken, lanes] = spun
+            raw = key[taken, mine].astype(jnp.float32)
+            full = (raw * cosine + swap_halves(raw, head_dim) * sine) * head_dim ** (-0.5)
+            keys = full.astype(half)
+            values = value[taken, mine]
+            sums = cum_lanes[taken, lanes]
+            total = total_lanes[pl.ds(pl.multiple_of(span * 8, 8), 8), lanes][0:1]
+
+            def attend(queries, column, head):
+                gaps = jnp.where(causal, column - cum_rows[head : head + 1, taken], -jnp.inf)
+                weights = (dot(queries, keys, 1, 1) * jnp.exp(gaps)).astype(half)
+                return dot(weights, values, 1, 0)
+
+            if narrow:
+                head = wide_groups + 2 * own
+                first = attend(jnp.where(low_half, spun, jnp.zeros_like(spun)), sums[:, 0:1], head)
+                second = attend(
+                    jnp.where(low_half, jnp.zeros_like(spun), spun), sums[:, 64:65], head + 1
+                )
+                within[taken, lanes] = jnp.where(low_half, first, second)
+            else:
+                within[taken, lanes] = attend(spun, sums, g)
+            scaled = (full * jnp.exp(total - sums)).astype(half)
+            update = dot(scaled, values, 0, 0)
+            if narrow:
+                update = jnp.where(same_head, update, 0.0)
+            old = state[g]
+            carried[span, g] = old
+            state[g] = old * jnp.exp(total) + update
+
+    prefix[...] = jnp.zeros_like(prefix)
+    prefix_decay[...] = jnp.ones_like(prefix_decay)
+
+    def state_copies(step):
+        device = (lax.rem(sp + distances[step], count_sp), tp)
+        return (
+            remote(
+                state_out.at[step], state_in.at[step],
+                state_send.at[step], state_recv.at[step], device,
+            ),
+            remote(
+                decay_out.at[step], decay_in.at[step],
+                decay_send.at[step], decay_recv.at[step], device,
+            ),
+        )
+
+    def send_state(step):
+        @pl.when(sp + distances[step] < count_sp)
+        def _():
+            for copy in state_copies(step):
+                copy.start()
+
+    def take_state(step):
+        @pl.when(sp >= distances[step])
+        def _():
+            for copy in state_copies(step):
+                copy.wait_recv()
+            for g in range(groups):
+                arrived = state_in[step, g].astype(jnp.float32)
+                decay = decay_in[step, g : g + 1, :]
+                prefix[g] = arrived * prefix_decay[g : g + 1, :] + prefix[g]
+                prefix_decay[g : g + 1, :] = decay * prefix_decay[g : g + 1, :]
+                if step + 1 < len(distances):
+                    mine = decay_out[step, g : g + 1, :]
+                    state[g] = arrived * mine + state[g]
+                    decay_out[step + 1, g : g + 1, :] = decay * mine
+                    state_out[step + 1, g] = state[g].astype(half)
+
+        if step + 1 < len(distances):
+            @pl.when(sp < distances[step])
+            def _():
+                decay_out[step + 1] = decay_out[step]
+                for g in range(groups):
+                    state_out[step + 1, g] = state[g].astype(half)
+
+            send_state(step + 1)
+
+    decay_out[0] = jnp.ones_like(decay_out[0])
+    for g in range(groups):
+        decay_out[0, g : g + 1, :] = device_lanes[:, g * 128 : (g + 1) * 128]
+        state_out[0, g] = state[g].astype(half)
+    send_state(0)
+    relay(0, 0, True)
+    begin(1)
+    for step in range(max(len(distances), line - 1)):
+        if step < len(distances):
+            take_state(step)
+        if step + 1 <= line - 2:
+            relay(0, step + 1, False)
+        elif step == line - 2:
+            relay(1, 0, True)
+
+    @pl.loop(0, length // SPAN)
+    def _(span):
+        taken = pl.ds(pl.multiple_of(span * SPAN, SPAN), SPAN)
+        for g, narrow, own in plans:
+            lanes, mine = slice(g * 128, (g + 1) * 128), slice(own * 128, (own + 1) * 128)
+            grown = jnp.exp(earlier_lanes[pl.ds(pl.multiple_of(span * 8, 8), 8), lanes][0:1])
+            entering = (prefix[g] * grown + carried[span, g]).astype(half)
+            across = dot(turned[taken, lanes], entering, 1, 0) * jnp.exp(cum_lanes[taken, lanes])
+            output = within[taken, lanes] + across
+            square = output * output
+            if narrow:
+                gate = narrow_gate[taken, mine].astype(jnp.float32)
+                first = jnp.sum(jnp.where(low_half, square, 0.0), axis=-1, keepdims=True)
+                second = jnp.sum(jnp.where(low_half, 0.0, square), axis=-1, keepdims=True)
+                mean = jnp.where(low_half, first, second) * (1.0 / NARROW_DIM)
+            else:
+                gate = wide_gate[taken, mine].astype(jnp.float32)
+                mean = jnp.mean(square, axis=-1, keepdims=True)
+            normed = output * lax.rsqrt(mean + epsilon)
+            mixed[taken, lanes] = (normed * (gate / (1.0 + jnp.exp(-gate)))).astype(half)
+
+    wide_lanes = wide_groups * 128
 
     def project(start):
         taken = pl.ds(pl.multiple_of(start * block_rows, block_rows), block_rows)
         return jnp.dot(
-            wide_mixed[taken, :], wide_out[...], preferred_element_type=jnp.float32
-        ) + jnp.dot(narrow_mixed[taken, :], narrow_out[...], preferred_element_type=jnp.float32)
+            mixed[taken, :wide_lanes], wide_out[...], preferred_element_type=jnp.float32
+        ) + jnp.dot(mixed[taken, wide_lanes:], narrow_out[...], preferred_element_type=jnp.float32)
 
     def part_copy(offset):
-        return pltpu.make_async_remote_copy(
-            src_ref=part_out.at[offset], dst_ref=part_in.at[offset],
-            send_sem=part_send.at[offset], recv_sem=part_recv.at[offset],
-            device_id=peer(offset), device_id_type=MESH,
+        return remote(
+            part_out.at[offset], part_in.at[offset],
+            part_send.at[offset], part_recv.at[offset], peer(offset),
         )
 
     @pl.loop(1, count_tp)
     def _(offset):
-        part_out[offset] = project(lax.rem(tp + offset, count_tp)).astype(jnp.bfloat16)
+        part_out[offset] = project(lax.rem(tp + offset, count_tp)).astype(half)
         part_copy(offset).start()
 
     lowered[...] = project(tp)
+    relay(1, 1, False)
     for offset in range(1, count_tp):
         part_copy(offset).wait_recv()
         lowered[...] += part_in[offset].astype(jnp.float32)
 
     mine = pl.ds(pl.multiple_of(tp * block_rows, block_rows), block_rows)
     moved = residual[...].astype(jnp.float32) + rms_scale(lowered[...], gain_mix[...])
-    moved = moved.astype(jnp.bfloat16)
+    moved = moved.astype(half)
     updated[...] = moved
-    rows[mine, :] = rms_scale(moved.astype(jnp.float32), gain_pre[...]).astype(jnp.bfloat16)
+    rows[mine, :] = rms_scale(moved.astype(jnp.float32), gain_pre[...]).astype(half)
 
     def row_copy(offset):
-        return pltpu.make_async_remote_copy(
-            src_ref=rows.at[mine], dst_ref=rows.at[mine],
-            send_sem=row_send.at[offset], recv_sem=row_recv.at[offset],
-            device_id=peer(offset), device_id_type=MESH,
+        return remote(
+            rows.at[mine], rows.at[mine], row_send.at[offset], row_recv.at[offset], peer(offset)
         )
 
     for offset in range(1, count_tp):
         row_copy(offset).start()
-    relay(0)
-    load_up.wait()
+    for place in range(line):
+        wait_pair(0, place)
     for offset in range(1, count_tp):
         row_copy(offset).wait_recv()
 
@@ -369,24 +578,27 @@
     @pl.loop(0, hidden.shape[1] // width)
     def _(tile):
         taken = pl.ds(pl.multiple_of(tile * width, width), width)
-        rectified = jax.nn.relu(
-            jnp.dot(rows[...], up_held[:, taken], preferred_element_type=jnp.float32)
-        )
-        hidden[:, taken] = (rectified * rectified).astype(jnp.bfloat16)
+        total = jnp.zeros((length, width), jnp.float32)
+        for block in range(count_sp):
+            total += jnp.dot(
+                rows[:, block * slab : (block + 1) * slab], up_slots[block, :, taken],
+                preferred_element_type=jnp.float32,
+            )
+        rectified = jax.nn.relu(total)
+        hidden[:, taken] = (rectified * rectified).astype(half)
 
     def low_copy(offset, block):
         start = lax.rem(tp + offset, count_tp) * block_rows
-        return pltpu.make_async_remote_copy(
-            src_ref=low_out.at[block, pl.ds(pl.multiple_of(start, block_rows), block_rows)],
-            dst_ref=low_in.at[offset, block],
-            send_sem=low_send.at[offset, block], recv_sem=low_recv.at[offset, block],
-            device_id=peer(offset), device_id_type=MESH,
+        return remote(
+            low_out.at[block, pl.ds(pl.multiple_of(start, block_rows), block_rows)],
+            low_in.at[offset, block],
+            low_send.at[offset, block], low_recv.at[offset, block], peer(offset),
         )
 
     def consume(block):
         low_out[block] = jnp.dot(
-            hidden[...], slots[block], preferred_element_type=jnp.float32
-        ).astype(jnp.bfloat16)
+            hidden[...], down_slots[block], preferred_element_type=jnp.float32
+        ).astype(half)
         for offset in range(1, count_tp):
             low_copy(offset, block).start()
 
@@ -400,15 +612,14 @@
             act(a + distance)
 
     def from_pair(place):
-        for index in range(PIECES):
-            pair_copy(index, place, 1 - b).wait_recv()
+        wait_pair(1, place)
         consume(place * 2 + 1 - b)
 
     @pl.loop(0, line)
     def _(distance):
-        @pl.when(distance + 1 <= line - 2)
+        @pl.when((distance + 1 <= line - 2) & (distance > 0))
         def _():
-            relay(distance + 1)
+            relay(1, distance + 1, False)
 
         at_distance(lambda place: consume(place * 2 + b), distance)
         at_distance(from_pair, distance)
@@ -422,7 +633,7 @@
         lowered[:, taken] = total
     result[...] = (
         updated[...].astype(jnp.float32) + rms_scale(lowered[...], gain_mlp[...])
-    ).astype(jnp.bfloat16)
+    ).astype(half)
 
     for offset in range(1, count_tp):
         part_copy(offset).wait_send()
@@ -432,40 +643,88 @@
         def _(block):
             low_copy(offset, block).wait_send()
 
-    for index in range(PIECES):
-        @pl.loop(0, line)
-        def _(place):
-            pair_copy(index, place, b).wait_send()
-
-        @pl.loop(0, line - 1)
-        def _(step):
-            @pl.when((a + 1 < line) & (a - step >= 0))
-            def _():
-                right_copy(step, index, jnp.maximum(a - step, 0)).wait_send()
-
-            @pl.when((a >= 1) & (a + step < line))
-            def _():
-                left_copy(step, index, jnp.minimum(a + step, line - 1)).wait_send()
-
-
-def tail_call(
-    wide_mixed, narrow_mixed, wide_out, narrow_out, residual,
-    gain_mix, gain_pre, gain_mlp, up_whole, down_weight, count_sp, count_tp,
+    for step in range(len(distances)):
+        @pl.when(sp + distances[step] < count_sp)
+        def _():
+            for copy in state_copies(step):
+                copy.wait_send()
+
+    for which in range(2):
+        swap_copy(which, a).wait_send()
+        for index in range(PIECES):
+            @pl.loop(0, line)
+            def _(place):
+                if index == 0:
+                    pair_copy(which, index, place, b).wait_send()
+                else:
+                    @pl.when(place != twin)
+                    def _():
+                        pair_copy(which, index, place, b).wait_send()
+
+            @pl.loop(0, line - 1)
+            def _(step):
+                @pl.when((a + 1 < line) & (a - step >= 0))
+                def _():
+                    right_copy(which, step, index, jnp.maximum(a - step, 0)).wait_send()
+
+                @pl.when((a >= 1) & (a + step < line))
+                def _():
+                    left_copy(which, step, index, jnp.minimum(a + step, line - 1)).wait_send()
+
+
+def turn_tables(head_dim, positions):
+    lane = jnp.arange(128, dtype=jnp.int32) % head_dim
+    half = head_dim // 2
+    pair = (lane % half).astype(jnp.float32) * 2.0
+    inverse = 10000.0 ** (-pair / head_dim)
+    angles = positions.astype(jnp.float32)[:, None] * inverse[None, :]
+    return jnp.cos(angles), jnp.where(lane < half, -1.0, 1.0)[None, :] * jnp.sin(angles)
+
+
+def whole_call(
+    wide, narrow, wide_decay, narrow_decay, residual, wide_out, narrow_out,
+    up_weight, down_weight, gain_mix, gain_pre, gain_mlp, count_sp, count_tp,
 ):
     block_rows, features = residual.shape
-    length = block_rows * count_tp
+    length = wide[0].shape[0]
+    spans = length // SPAN
+    slab, inner = up_weight.shape
     depth, columns = down_weight.shape
-    half, line = jnp.bfloat16, count_sp // 2
+    wide_groups, narrow_groups = wide[0].shape[1] // 128, narrow[0].shape[1] // 128
+    groups = wide_groups + narrow_groups
+    positions = lax.axis_index("sp") * length + jnp.arange(length, dtype=jnp.int32)
+    tables = jnp.stack([*turn_tables(WIDE_DIM, positions), *turn_tables(NARROW_DIM, positions)])
+    decay = jnp.concatenate([wide_decay, narrow_decay], axis=0)
+    heads = decay.shape[0]
+    cumulative = jnp.cumsum(decay.reshape(heads, spans, SPAN), axis=-1)
+    cum_rows = cumulative.reshape(heads, length)
+    widths = [WIDE_DIM] * wide_decay.shape[0] + [NARROW_DIM] * narrow_decay.shape[0]
+
+    def over_lanes(values):
+        return jnp.concatenate(
+            [
+                jnp.broadcast_to(values[:, h : h + 1], (values.shape[0], width))
+                for h, width in enumerate(widths)
+            ],
+            axis=1,
+        )
+
+    totals = cumulative[:, :, -1].T
+    earlier = jnp.cumsum(totals, axis=0) - totals
+    device = jnp.exp(jnp.sum(totals, axis=0, keepdims=True))
+    half, full, line = jnp.bfloat16, jnp.float32, count_sp // 2
+    steps = (count_sp - 1).bit_length()
+    tall = -(-groups // 8) * 8
     dma = pltpu.SemaphoreType.DMA
     vmem = pl.BlockSpec(memory_space=pltpu.VMEM)
     anywhere = pl.BlockSpec(memory_space=pl.ANY)
     return pl.pallas_call(
-        functools.partial(tail_kernel, count_sp, count_tp),
+        functools.partial(whole_kernel, count_sp, count_tp, wide_groups, narrow_groups),
         out_shape=jax.ShapeDtypeStruct(residual.shape, half),
-        in_specs=[vmem] * 8 + [anywhere] * 2,
+        in_specs=[vmem] * 20 + [anywhere] * 2,
         out_specs=vmem,
         scratch_shapes=[
-            pltpu.VMEM(up_whole.shape, half),
+            pltpu.VMEM((count_sp, slab, inner), half),
             pltpu.VMEM((count_sp, depth, columns), half),
             pltpu.VMEM((count_tp, block_rows, features), half),
             pltpu.VMEM((count_tp, block_rows, features), half),
@@ -474,25 +733,44 @@
             pltpu.VMEM((count_sp, length, columns), half),
             pltpu.VMEM((count_tp, count_sp, block_rows, columns), half),
             pltpu.VMEM((block_rows, features), half),
-            pltpu.VMEM((block_rows, features), jnp.float32),
-            dma((2, line - 1, PIECES)),
-            dma((2, line - 1, PIECES)),
-            dma((line, PIECES)),
-            dma((line, PIECES)),
+            pltpu.VMEM((block_rows, features), full),
+            pltpu.VMEM((length, groups * 128), half),
+            pltpu.VMEM((length, groups * 128), full),
+            pltpu.VMEM((spans, groups, 128, 128), full),
+            pltpu.VMEM((length, groups * 128), half),
+            pltpu.VMEM((groups, 128, 128), full),
+            pltpu.VMEM((groups, 128, 128), full),
+            pltpu.VMEM((tall, 128), full),
+            pltpu.VMEM((steps, groups, 128, 128), half),
+            pltpu.VMEM((steps, groups, 128, 128), half),
+            pltpu.VMEM((steps, tall, 128), full),
+            pltpu.VMEM((steps, tall, 128), full),
+            dma((2, 2, line - 1, PIECES)),
+            dma((2, 2, line - 1, PIECES)),
+            dma((2, line, PIECES)),
+            dma((2, line, PIECES)),
+            dma((2,)),
+            dma((2,)),
             dma((count_tp,)),
             dma((count_tp,)),
             dma((count_tp,)),
             dma((count_tp,)),
             dma((count_tp, count_sp)),
             dma((count_tp, count_sp)),
+            dma((steps,)),
+            dma((steps,)),
+            dma((steps,)),
+            dma((steps,)),
             dma((2,)),
         ],
         compiler_params=pltpu.CompilerParams(
-            collective_id=0, has_side_effects=True, vmem_limit_bytes=52 * 1024 * 1024
+            collective_id=0, has_side_effects=True, vmem_limit_bytes=58 * 1024 * 1024
         ),
     )(
-        wide_mixed, narrow_mixed, wide_out, narrow_out, residual,
-        gain_mix[None, :], gain_pre[None, :], gain_mlp[None, :], up_whole, down_weight,
+        *wide, *narrow, tables, cum_rows, over_lanes(cum_rows.T),
+        jnp.repeat(over_lanes(totals), 8, axis=0), jnp.repeat(over_lanes(earlier), 8, axis=0),
+        over_lanes(device), residual, wide_out, narrow_out,
+        gain_mix[None, :], gain_pre[None, :], gain_mlp[None, :], up_weight, down_weight,
     )
 
 

time: 252 us -> 215 us (0.85); the launches traced: 248 us -> 215 us
  Pallas kernels: 102 us -> 199 us
  waiting for transfers between devices: 58.3 us -> 0 us
  local copies, waits for them, and re-layouts: 31.7 us -> 10.5 us
  other arithmetic: 24.8 us -> 5.46 us
  between operations: 13.9 us -> 0.13 us
  matrix products: 11.5 us -> 0 us
  starting transfers between devices: 5.88 us -> 0 us
    pallas_call x1, Pallas kernels: 102 us -> 199 us  [whole_call(): pl.pallas_call(functools.partial(whole_kernel, count_sp, count_tp, wide_g...]
    all_gather x1 -> x0, waiting for transfers between devices: 39.8 us -> none  [local(): up_whole = lax.all_gather(up_weight, 'sp', axis=0, tiled=True)]
    ppermute x3 -> x0, waiting for transfers between devices: 17.8 us -> none  [earlier_states(): lax.ppermute(pack_states(whole), axis, [(i, i + distance) for i in range(...]
    dot_general x6 -> x0, matrix products: 11.5 us -> none  [the longest x2 4.9 us: finish(): jnp.einsum('nihd,nhde->nihe', queries, entering, preferred_element_type=j...]
    mul x22 -> x0, local copies, waits for them, and re-layouts: 10.6 us -> none  [the longest x10 3.8 us: advance(): return (carried * jnp.exp(decay_sum)[:, None, None] + contribution, carried)]
    ppermute x3 -> x0, starting transfers between devices: 5.87 us -> none  [earlier_states(): lax.ppermute(pack_states(whole), axis, [(i, i + distance) for i in range(...]
    unnamed x39 -> x4, local copies, waits for them, and re-layouts: 6.68 us -> 1.89 us
    another operation x14 -> x3, other arithmetic: 7.28 us -> 2.62 us  [the longest x1 1.52 us: whole_call(): cumulative = jnp.cumsum(decay.reshape(heads, spans, SPAN), axis=-1)]
  transfers between devices with their start and end apart: 4 -> 0, of which waited for: 4 -> 0; matrix products, arithmetic and copies ran while one was open for 27% -> 0% of each run, Pallas kernels for 0% -> 0%
where the time goes in v2:
time: 215 us
  Pallas kernels  199 us (93%)
  local copies, waits for them, and re-layouts  10.5 us (5%)
  other arithmetic  5.46 us (3%)
    pallas_call x1, Pallas kernels, whole_call(): pl.pallas_call(functools.partial(whole_kernel, count_sp, count_tp, wide_g...  199 us
    broadcast_in_dim x20, local copies, waits for them, and re-layouts, over_lanes(): jnp.broadcast_to(values[:, h:h + 1], (values.shape[0], width))  4.48 us

profile of v2, /device:TPU:25, one launch (start us, length us, event | category | flops | bytes accessed | tf_op | source)
XLA Modules:
  0.0 214.8 jit_solution(484943112574810026)
XLA Ops:
  0.0 0.7 pad_maximum_fusion.1
  0.8 1.5 reduce_window_sum.22
  2.3 0.2 slice_reduce_fusion.10
  2.5 0.1 copy.20
  2.7 0.3 slice_reduce_fusion
  2.9 0.1 broadcast_in_dim.204
  3.0 0.1 broadcast_in_dim.202
  3.1 0.1 broadcast_in_dim.200
  3.1 0.1 broadcast_in_dim.198
  3.2 0.1 broadcast_in_dim.196
  3.3 0.1 concatenate.18
  3.4 0.7 fusion.16
  4.0 0.6 broadcast_in_dim.215
  4.7 0.7 broadcast_in_dim.213
  5.4 0.6 broadcast_in_dim.211
  5.9 0.6 broadcast_in_dim.209
  6.6 0.6 broadcast_in_dim.207
  7.2 0.7 concatenate.19.device_lanes
  7.9 0.2 slice_reduce_fusion.5
  8.2 0.1 broadcast_in_dim.193
  8.2 0.1 broadcast_in_dim.191
  8.3 0.1 broadcast_in_dim.189
  8.4 0.1 broadcast_in_dim.187
  8.4 0.1 broadcast_in_dim.185
  8.5 0.1 concatenate.17
  8.6 0.0 copy-start
  8.6 0.6 broadcast_bitcast_fusion
  9.3 0.1 broadcast_in_dim.181
  9.4 0.1 broadcast_in_dim.183
  9.5 0.1 broadcast_in_dim.179
  9.7 0.1 broadcast_in_dim.177
  9.8 0.1 broadcast_in_dim.175
  10.0 1.3 concatenate.16.cum_lanes
  11.2 0.0 copy-done
  11.2 1.9 multiply_cosine_fusion.1
  13.1 1.1 pad_maximum_fusion.tables
  14.2 198.7 %shard_map.172 = bf16[128,2048]{1,0:T(8,128)(2,1)} custom-call(bf16[512,384]{1,0:T(8,128)(2,1)} %wide_query.1, bf16[512,384]{1,0:T(8,128)(2,1)} %wide_key.1, bf16[512,384]{1,0:T(8,128)(2,1)} %wide_value.1, bf16[512,384]{1,0:T(8,128)(2,1)} %wide_gate.1, bf16[512,128]{1,0:T(8,128)(2,1)} %narrow_query.1, bf16[512,128]{1,0:T(8,128)(2,1)} %narrow_key.1, ...), custom_call_target="tpu_custom_call" | custom-call | tf_op jit(solution)/shard_map/pallas_call | solution.py:721
  212.9 1.9 copy.27
  (9 shorter events, 0.1 us)
Async XLA Ops:
  8.6 2.6 %copy-start = (f32[1,5,4,128]{3,1,2,0:T(8,128)}, f32[1,5,4,128]{3,1,2,0:T(8,128)S(1)}, u32[]{:S(2)}) copy-start(f32[1,5,4,128]{3,1,2,0:T(8,128)S(1)} %copy.25) | copy-start | bytes 30724

commit v3 on v2

--- a/solution.py
+++ b/solution.py
@@ -700,18 +700,15 @@
     cum_rows = cumulative.reshape(heads, length)
     widths = [WIDE_DIM] * wide_decay.shape[0] + [NARROW_DIM] * narrow_decay.shape[0]
 
+    owner = [h for h, width in enumerate(widths) for _ in range(width)]
+    spread = (jnp.arange(heads)[:, None] == jnp.array(owner)[None, :]).astype(jnp.float32)
+
     def over_lanes(values):
-        return jnp.concatenate(
-            [
-                jnp.broadcast_to(values[:, h : h + 1], (values.shape[0], width))
-                for h, width in enumerate(widths)
-            ],
-            axis=1,
-        )
+        return jnp.dot(values, spread, precision=lax.Precision.HIGHEST)
 
     totals = cumulative[:, :, -1].T
     earlier = jnp.cumsum(totals, axis=0) - totals
-    device = jnp.exp(jnp.sum(totals, axis=0, keepdims=True))
+    device = jnp.sum(totals, axis=0, keepdims=True)
     half, full, line = jnp.bfloat16, jnp.float32, count_sp // 2
     steps = (count_sp - 1).bit_length()
     tall = -(-groups // 8) * 8
@@ -768,8 +765,8 @@
         ),
     )(
         *wide, *narrow, tables, cum_rows, over_lanes(cum_rows.T),
-        jnp.repeat(over_lanes(totals), 8, axis=0), jnp.repeat(over_lanes(earlier), 8, axis=0),
-        over_lanes(device), residual, wide_out, narrow_out,
+        over_lanes(jnp.repeat(totals, 8, axis=0)), over_lanes(jnp.repeat(earlier, 8, axis=0)),
+        jnp.exp(over_lanes(device)), residual, wide_out, narrow_out,
         gain_mix[None, :], gain_pre[None, :], gain_mlp[None, :], up_weight, down_weight,
     )
 

time: 215 us -> 210 us (0.977)
  local copies, waits for them, and re-layouts: 10.5 us -> 3.23 us
  matrix products: 0 us -> 3.36 us
    broadcast_in_dim x20 -> x0, local copies, waits for them, and re-layouts: 4.48 us -> none  [over_lanes(): jnp.broadcast_to(values[:, h:h + 1], (values.shape[0], width))]
    dot_general x0 -> x4, matrix products: none -> 3.36 us  [over_lanes(): return jnp.dot(values, spread, precision=lax.Precision.HIGHEST)]
where the time goes in v3:
time: 210 us
  Pallas kernels  199 us (95%)
  other arithmetic  4.76 us (2%)
  matrix products  3.36 us (2%)
  local copies, waits for them, and re-layouts  3.23 us (2%)
    pallas_call x1, Pallas kernels, whole_call(): pl.pallas_call(functools.partial(whole_kernel, count_sp, count_tp, wide_g...  199 us

profile of v3, /device:TPU:25, one launch (start us, length us, event | category | flops | bytes accessed | tf_op | source)
XLA Modules:
  0.0 210.1 jit_solution(6309253427909267828)
XLA Ops:
  0.0 0.0 copy-start.1
  0.0 0.0 copy-start.2
  0.1 0.0 copy-start
  0.1 1.9 multiply_cosine_fusion.1
  2.0 1.1 pad_maximum_fusion.tables
  3.0 0.0 copy-done.1
  3.0 0.0 copy-done.2
  3.1 1.5 reduce_window_sum.22
  4.6 0.2 slice_reduce_fusion
  4.8 0.1 copy.20
  4.9 0.0 copy-done
  5.0 0.8 fusion.2.earlier_lanes
  5.7 0.8 fusion.4.total_lanes
  6.5 1.7 fusion.7.cum_lanes
  8.2 0.6 copy.24
  8.8 0.1 fusion.6
  8.9 0.6 exp.5
  9.5 198.7 %shard_map.181 = bf16[128,2048]{1,0:T(8,128)(2,1)} custom-call(bf16[512,384]{1,0:T(8,128)(2,1)} %wide_query.1, bf16[512,384]{1,0:T(8,128)(2,1)} %wide_key.1, bf16[512,384]{1,0:T(8,128)(2,1)} %wide_value.1, bf16[512,384]{1,0:T(8,128)(2,1)} %wide_gate.1, bf16[512,128]{1,0:T(8,128)(2,1)} %narrow_query.1, bf16[512,128]{1,0:T(8,128)(2,1)} %narrow_key.1, ...), custom_call_target="tpu_custom_call" | custom-call | tf_op jit(solution)/shard_map/pallas_call | solution.py:718
  208.3 1.9 copy.26
  (7 shorter events, 0.1 us)
Async XLA Ops:
  0.0 3.0 %copy-start.1 = (f32[3,512]{1,0:T(4,128)S(1)}, f32[3,512]{1,0:T(4,128)}, u32[]{:S(2)}) copy-start(f32[3,512]{1,0:T(4,128)} %param.27) | copy-start | bytes 18436
  0.0 3.0 %copy-start.2 = (f32[2,512]{1,0:T(2,128)S(1)}, f32[2,512]{1,0:T(2,128)}, u32[]{:S(2)}) copy-start(f32[2,512]{1,0:T(2,128)} %param.28) | copy-start | bytes 12292
  0.1 4.9 %copy-start = (s32[512]{0:T(512)S(1)}, s32[512]{0:T(512)}, u32[]{:S(2)}) copy-start(s32[512]{0:T(512)} %constant.78.clone) | copy-start | bytes 6148
